TPU v7x, 512 devices: a whole 4x8x8 slice. The times are simulated.
512 devices in a mesh: rep: 2 (over z_hi), fs: 32 (over z_lo, y), tp: 8 (over x, core).
Axes of the slice: x: 4, y: 8, z: 8 (z_hi: 2, z_lo: 4; z = z_hi * 4 + z_lo), core: 2. Of those that a mesh axis runs over, the one named last changes fastest.
Arguments:
- tokens: bfloat16 [8192, 2048], P(('rep', 'fs')), may hold values from -6 to 6
- attention_norm_gain: float32 [2048], replicated, may hold values from 0.1 to 1.9
- query_weight: bfloat16 [2048, 1024], P('fs', 'tp'), may hold values from -0.125 to 0.125
- key_weight: bfloat16 [2048, 1024], P('fs', 'tp'), may hold values from -0.125 to 0.125
- value_weight: bfloat16 [2048, 2048], P('fs', 'tp'), may hold values from -0.125 to 0.125
- decay_weight: bfloat16 [2048, 1024], P('fs', 'tp'), may hold values from -0.125 to 0.125
- decay_gate_bias: float32 [1024], P('tp'), may hold values from -1.5 to 5.5
- decay_spike_extra: float32 [8192, 32], P(('rep', 'fs'), 'tp'), may hold values from -0.7 to 0
- head_output_gain: float32 [64], replicated, may hold values from 0.1 to 1.9
- output_weight: bfloat16 [2048, 2048], P('fs', 'tp'), may hold values from -0.125 to 0.125
- channel_norm_gain: float32 [2048], replicated, may hold values from 0.1 to 1.9
- gate_weight: bfloat16 [2048, 3072], P('fs', 'tp'), may hold values from -0.125 to 0.125
- up_weight: bfloat16 [2048, 3072], P('fs', 'tp'), may hold values from -0.125 to 0.125
- down_weight: bfloat16 [2048, 3072], P('fs', 'tp'), may hold values from -0.109375 to 0.109375
Outputs:
- layer_out: bfloat16 [8192, 2048], P(('rep', 'fs'))
All inputs are finite; a program needn't handle non-finite values.
Results may differ from a plain program's by a relative error of at most 0.018.
Values may be sent and summed in bfloat16 or wider, within the bound.
A program may use at most 64 MiB of HBM per device.

v0:
```python
import jax
import jax.numpy as jnp
from jax import lax
from jax.sharding import PartitionSpec as P

BLOCK = 64


GATE_NORM = 16.0
NORM_EPS = 1e-06
HIGHEST = lax.Precision.HIGHEST


def sent_together(arrays, axis, dim, along):
    both = jnp.concatenate(arrays, axis=along)
    filled, at, outs = (lax.all_gather(both, axis, axis=dim, tiled=True), 0, [])
    for a in arrays:
        outs.append(lax.slice_in_dim(filled, at, at + a.shape[along], axis=along))
        at += a.shape[along]
    return tuple(outs)


def gathered_total(array, axis):
    return lax.all_gather(array, axis).astype(jnp.float32).sum(0)


def rms_scale(values, scales):
    floats = values.astype(jnp.float32)
    return floats * lax.rsqrt(jnp.mean(floats * floats, axis=-1, keepdims=True) + NORM_EPS) * scales


def one_way(queries, key_rows, value_rows, decay_logarithm):
    length, number_of_heads, key_width = queries.shape
    value_width = value_rows.shape[2]
    block_count = length // BLOCK

    def blocks(tensor):
        return tensor.reshape(block_count, BLOCK, number_of_heads, tensor.shape[2]).transpose(
            0, 2, 1, 3
        )

    lower_mask = jnp.tril(jnp.ones((BLOCK, BLOCK), bool))

    def advance(carried, pieces):
        query_part, key_part, value_part, decay_part = pieces
        running = jnp.cumsum(decay_part, axis=1)
        spread = jnp.where(
            lower_mask[None, :, :, None], running[:, :, None, :] - running[:, None, :, :], -jnp.inf
        )
        scores = jnp.einsum(
            "hid,hjd,hijd->hij", query_part, key_part, jnp.exp(spread), precision=HIGHEST
        )
        block_end = running[:, -1:, :]
        result = jnp.einsum("hij,hje->hie", scores, value_part, precision=HIGHEST)
        result = result + jnp.einsum(
            "hid,hde->hie", query_part * jnp.exp(running), carried, precision=HIGHEST
        )
        carried = jnp.exp(block_end)[:, 0, :, None] * carried + jnp.einsum(
            "hjd,hje->hde", key_part * jnp.exp(block_end - running), value_part, precision=HIGHEST
        )
        return (carried, result)

    zero_state = jnp.zeros((number_of_heads, key_width, value_width), jnp.float32)
    _, outputs = lax.scan(
        advance,
        zero_state,
        (blocks(queries), blocks(key_rows), blocks(value_rows), blocks(decay_logarithm)),
    )
    return outputs.transpose(0, 2, 1, 3).reshape(length, number_of_heads, value_width)


def both_ways(queries, key_rows, value_rows, decay_logarithm):
    forward = one_way(queries, key_rows, value_rows, decay_logarithm)
    backward = one_way(
        jnp.flip(queries, 0),
        jnp.flip(key_rows, 0),
        jnp.flip(value_rows, 0),
        jnp.flip(decay_logarithm, 0),
    )
    return forward + jnp.flip(backward, 0)


def rounded(floats):
    return lax.optimization_barrier(floats.astype(jnp.bfloat16)).astype(jnp.float32)


def shards(
    tokens,
    attention_norm_gain,
    query_weight,
    key_weight,
    value_weight,
    decay_weight,
    decay_gate_bias,
    decay_spike_extra,
    head_output_gain,
    output_weight,
    channel_norm_gain,
    gate_weight,
    up_weight,
    down_weight,
):
    full_query, full_key, full_value, full_decay, full_output, full_gate, full_up, full_down = (
        sent_together(
            (
                query_weight,
                key_weight,
                value_weight,
                decay_weight,
                output_weight,
                gate_weight,
                up_weight,
                down_weight,
            ),
            "fs",
            0,
            1,
        )
    )
    normed = rms_scale(tokens, attention_norm_gain).astype(jnp.bfloat16)
    narrow = full_query.shape[1]
    wide_cols = full_value.shape[1]
    length = normed.shape[0]
    number_of_heads = decay_spike_extra.shape[1]
    key_width = narrow // number_of_heads
    value_width = wide_cols // number_of_heads
    query_proj = jnp.dot(normed, full_query, preferred_element_type=jnp.float32)
    key_proj = jnp.dot(normed, full_key, preferred_element_type=jnp.float32)
    value_proj = jnp.dot(normed, full_value, preferred_element_type=jnp.float32)
    gate_pre = jnp.dot(normed, full_decay, preferred_element_type=jnp.float32)
    queries = (rounded(query_proj) * key_width ** (-0.5)).reshape(
        length, number_of_heads, key_width
    )
    key_rows = rounded(key_proj).reshape(length, number_of_heads, key_width)
    value_rows = rounded(value_proj).reshape(length, number_of_heads, value_width)
    decay_logarithm = (
        jax.nn.log_sigmoid(gate_pre + decay_gate_bias).reshape(length, number_of_heads, key_width)
        / GATE_NORM
    )
    decay_logarithm = decay_logarithm + decay_spike_extra[:, :, None]
    mixed_heads = both_ways(queries, key_rows, value_rows, decay_logarithm)
    attended = (
        rms_scale(mixed_heads, head_output_gain).reshape(length, wide_cols).astype(jnp.bfloat16)
    )
    mixer_term = lax.dot_general(
        attended, full_output, (((1,), (1,)), ((), ())), preferred_element_type=jnp.float32
    )
    mixed_sum = gathered_total(mixer_term.astype(jnp.bfloat16), "tp").astype(jnp.float32)
    residual = (tokens.astype(jnp.float32) + mixed_sum).astype(jnp.bfloat16)
    normed_two = rms_scale(residual, channel_norm_gain).astype(jnp.bfloat16)
    gate_part = jnp.dot(normed_two, full_gate, preferred_element_type=jnp.float32)
    up_part = jnp.dot(normed_two, full_up, preferred_element_type=jnp.float32)
    hidden = (jax.nn.silu(gate_part) * up_part).astype(jnp.bfloat16)
    channel_term = lax.dot_general(
        hidden, full_down, (((1,), (1,)), ((), ())), preferred_element_type=jnp.float32
    )
    channel_sum = gathered_total(channel_term.astype(jnp.bfloat16), "tp").astype(jnp.float32)
    return (residual.astype(jnp.float32) + channel_sum).astype(jnp.bfloat16)


def solution(mesh):
    in_specs = (
        P(("rep", "fs"), None),
        P(),
        P("fs", "tp"),
        P("fs", "tp"),
        P("fs", "tp"),
        P("fs", "tp"),
        P("tp"),
        P(("rep", "fs"), "tp"),
        P(),
        P("fs", "tp"),
        P(),
        P("fs", "tp"),
        P("fs", "tp"),
        P("fs", "tp"),
    )
    out_specs = P(("rep", "fs"), None)
    return jax.shard_map(shards, mesh=mesh, in_specs=in_specs, out_specs=out_specs, check_vma=False)
```

profile of v0, /device:TPU:1, one launch (start us, length us, event | category | flops | bytes accessed | tf_op | source)
XLA Modules:
  0.0 343.8 jit_solution(7419534605140882500)
XLA Ops:
  15.5 152.0 %all-gather.6.cloned.1.call-done = bf16[2048,2048]{1,0:T(8,128)(2,1)} async-done(((bf16[64,2048]{1,0:T(8,128)(2,1)}), bf16[2048,2048]{1,0:T(8,128)(2,1)}) %all-gather.6.cloned.1.call-update) | async-done | bytes 8388624 | tf_op jit(solution)/shard_map/all_gather | solution.py:16
  167.6 1.8 convolution_convert_fusion.2
  171.8 1.5 fusion.70
  175.6 27.5 %while.27 = (s32[]{:T(128)}, f32[4,32,64]{2,1,0:T(8,128)S(1)}, f32[2,4,64,64]{3,2,1,0:T(8,128)S(1)}, f32[2,4,64,32]{2,0,3,1:T(2,128)S(1)}, f32[2,4,64,32]{2,0,3,...) while((s32[]{:T(128)}, f32[4,32,64]{2,1,0:T(8,128)S(1)}, ...), condition=%wide.region_6.7_spmd.clone, body=%wide.region_4.6_spmd.clone.sunk | while | flops 28364804 | bytes 10234500 | solution.py:64
  176.0 3.1 select_exponential_fusion.5
  179.1 5.8 %copy.149 = f32[4,64,64,32]{1,2,3,0:T(8,128)} copy(f32[4,64,64,32]{2,3,1,0:T(8,128)} %select_exponential_fusion.5) | data formatting | bytes 4194304 | tf_op jit(solution)/shard_map/while
  185.0 2.9 fusion.110
  189.8 3.1 select_exponential_fusion.5
  192.9 5.8 %copy.149 = f32[4,64,64,32]{1,2,3,0:T(8,128)} copy(f32[4,64,64,32]{2,3,1,0:T(8,128)} %select_exponential_fusion.5) | data formatting | bytes 4194304 | tf_op jit(solution)/shard_map/while
  198.8 2.9 fusion.110
  203.9 26.9 %while.26 = (s32[]{:T(128)}, f32[4,32,64]{2,1,0:T(8,128)S(1)}, f32[2,4,64,64]{3,2,1,0:T(8,128)S(1)}, f32[2,4,64,32]{3,2,1,0:T(8,128)S(1)}, f32[2,4,64,32]{2,0,3,...) while((s32[]{:T(128)}, f32[4,32,64]{2,1,0:T(8,128)S(1)}, ...), condition=%wide.region_3.4_spmd.clone, body=%wide.region_1.3_spmd.clone.sunk | while | flops 28364804 | bytes 10466952 | solution.py:64
  204.2 3.1 select_exponential_fusion.4
  207.3 5.8 %copy.144 = f32[4,64,64,32]{1,2,3,0:T(8,128)} copy(f32[4,64,64,32]{2,3,1,0:T(8,128)} %select_exponential_fusion.4) | data formatting | bytes 4194304 | tf_op jit(solution)/shard_map/while
  213.2 2.9 fusion.103
  217.7 3.1 select_exponential_fusion.4
  220.8 5.8 %copy.144 = f32[4,64,64,32]{1,2,3,0:T(8,128)} copy(f32[4,64,64,32]{2,3,1,0:T(8,128)} %select_exponential_fusion.4) | data formatting | bytes 4194304 | tf_op jit(solution)/shard_map/while
  226.7 2.9 fusion.103
  231.4 2.5 convolution_convert_fusion.1
  234.1 52.8 %all-gather.8.cloned.1.call-done = bf16[1024,2048]{1,0:T(8,128)(2,1)} async-done(((bf16[128,2048]{1,0:T(8,128)(2,1)}), bf16[1024,2048]{1,0:T(8,128)(2,1)}) %all-gather.8.cloned.1.call-update) | async-done | bytes 4194320 | tf_op jit(solution)/shard_map/all_gather | solution.py:24
  286.9 3.0 convert_reduce_fusion.1
  290.2 1.9 fusion.36
  292.1 3.7 %convolution_convert_fusion = bf16[128,2048]{1,0:T(8,128)(2,1)} fusion(bf16[2048,2048]{1,0:T(8,128)(2,1)} %all-gather.6.cloned.1.call-done, f32[128,384]{1,0:T(8,128)S(1)} %fusion.36, bf16[128,2048]{1,0:T(8,128)(2,1)S(1)} %get-tuple-element.214, f32[2048]{0:T(1024)S(1)} %copy-done.5, f32[128]{0:T(128)S(1)} %add_rsqrt_fusion.1), kind=kOutput, calls=%fused_computation.56 | convolution fusion | flops 404258816 | bytes 4399616 | tf_op jit(solution)/shard_map/dot_general | solution.py:154
  295.8 37.5 %all-gather.10.cloned.1.call-done = bf16[1024,2048]{1,0:T(8,128)(2,1)} async-done(((bf16[128,2048]{1,0:T(8,128)(2,1)}), bf16[1024,2048]{1,0:T(8,128)(2,1)}) %all-gather.10.cloned.1.call-update) | async-done | bytes 4194320 | tf_op jit(solution)/shard_map/all_gather | solution.py:24
  333.4 3.0 convert_reduce_fusion
  (117 shorter events, 23.3 us)
Async XLA Ops:
  6.5 163.4 %copy-start = (bf16[128,2048]{1,0:T(8,128)(2,1)S(1)}, bf16[128,2048]{1,0:T(8,128)(2,1)}, u32[]{:S(2)}) copy-start(bf16[128,2048]{1,0:T(8,128)(2,1)} %param.18) | copy-start | bytes 1572868
  6.5 163.4 %copy-start.4 = (f32[2048]{0:T(1024)S(1)}, f32[2048]{0:T(1024)}, u32[]{:S(2)}) copy-start(f32[2048]{0:T(1024)} %param.19) | copy-start | bytes 24580
  6.5 165.3 %copy-start.6 = (f32[128]{0:T(128)S(1)}, f32[128]{0:T(128)}, u32[]{:S(2)}) copy-start(f32[128]{0:T(128)} %param.24) | copy-start | bytes 1540
  6.5 161.1 %all-gather.6.cloned.1.call-start = ((), (), s32[]{:S(2)}) async-start(), calls=%async_computation | async-start | bytes 8650752 | tf_op jit(solution)/shard_map/all_gather | solution.py:16
  12.7 0.7 copy-start.1
  13.5 160.0 %copy-start.2 = (f32[128,4]{0,1:T(4,128)S(1)}, f32[128,4]{0,1:T(4,128)}, u32[]{:S(2)}) copy-start(f32[128,4]{0,1:T(4,128)} %param.25) | copy-start | bytes 6148
  13.5 273.4 %all-gather.8.cloned.1.call-start = ((), (), s32[]{:S(2)}) async-start(), calls=%async_computation.1 | async-start | bytes 4718592 | tf_op jit(solution)/shard_map/all_gather | solution.py:24
  203.9 27.3 %copy-start.3 = (f32[64]{0:T(128)S(1)}, f32[64]{0:T(128)}, u32[]{:S(2)}) copy-start(f32[64]{0:T(128)} %param.26) | copy-start | bytes 772
  233.9 56.3 %copy-start.5 = (f32[2048]{0:T(1024)S(1)}, f32[2048]{0:T(1024)}, u32[]{:S(2)}) copy-start(f32[2048]{0:T(1024)} %param.28) | copy-start | bytes 24580
  233.9 99.5 %all-gather.10.cloned.1.call-start = ((), (), s32[]{:S(2)}) async-start(), calls=%async_computation.2 | async-start | bytes 4718592 | tf_op jit(solution)/shard_map/all_gather | solution.py:24
Sparse Core Ops, SparseCore 0:
  13.6 153.9 all-gather.5
  234.0 52.8 all-gather.7
  295.9 37.3 all-gather.9
where the time goes:
time: 345 us; the launch traced here: 344 us
  waiting for transfers between devices  242 us (70%)
  local copies, waits for them, and re-layouts  35.9 us (10%)
  other arithmetic  33 us (10%)
  matrix products  18.3 us (5%)
  between operations  13.4 us (4%)
    all_gather x1, waiting for transfers between devices, sent_together(): filled, at, outs = (lax.all_gather(both, axis, axis=dim, tiled=True), 0, [])  152 us
    all_gather x2, waiting for transfers between devices, gathered_total(): return lax.all_gather(array, axis).astype(jnp.float32).sum(0)  90.3 us
    while x4, local copies, waits for them, and re-layouts  23.2 us
    exp x4, other arithmetic, advance(): jnp.exp(spread)  12.3 us
    dot_general x4, other arithmetic, advance(): jnp.einsum('hid,hjd,hijd->hij', query_part, key_part, jnp.exp(spread), pr...  11.4 us
  transfers between devices with their start and end apart: 3, of which 3 were waited for; matrix products, arithmetic and copies ran while one was open for 1% of the time, Pallas kernels for 0%

commit v1 on v0

v1 whole, which is shorter than its diff:
```python
import functools

import jax
import jax.numpy as jnp
from jax import lax
from jax.experimental import pallas as pl
from jax.experimental.pallas import tpu as pltpu
from jax.sharding import PartitionSpec as P

MESH = pl.DeviceIdType.MESH
F32, BF16 = jnp.float32, jnp.bfloat16
NY, NZ, NTP = 8, 4, 8
SEQ, D = 128, 2048
SLAB = D // (NY * NZ)
HEADS, KW, VW = 4, 32, 64
LEVELS = 7
EPS = 1e-6
PARTS = ((128, 128, 256, 128), (256,), (384, 384), (384,))
A_ROWS = (((0, 16), (16, 16)),) * 4
B_ROWS = (((32, 16), (48, 16)),) * 4
ROWS_OWN = SEQ // NTP


def dot(a, b):
    return jnp.dot(a, b, preferred_element_type=F32)


def dot_t(a, b):
    return lax.dot_general(a, b, (((1,), (1,)), ((), ())), preferred_element_type=F32)


def iota(shape, axis):
    return lax.broadcasted_iota(jnp.int32, shape, axis)


def layer_kernel(
    tok, gain1, bias, spike, hgain, gain2, wq, wk, wv, wd, wo, wg, wu, wdn,
    out,
    g1, g2, g3, g4, xn, acc, mats, score, att, part, got, n2, acc2, hid, part2, got2, resid, decay2, qf, kf, vbd,
    lsem, send, recv, tsend, trecv,
):
    bufs = (g1, g2, g3, g4)
    rep, f, t = lax.axis_index("rep"), lax.axis_index("fs"), lax.axis_index("tp")
    y, z = lax.rem(f, NY), lax.div(f, NY)
    zz = rep * NZ + z

    def at_y(k):
        return (rep, z * NY + lax.rem(y + k + NY, NY), t)

    def at_z(k):
        w = lax.rem(zz + k + 2 * NZ, 2 * NZ)
        return (lax.div(w, NZ), lax.rem(w, NZ) * NY + y, t)

    ynb, znb = (at_y(1), at_y(-1)), (at_z(1), at_z(-1))

    def peer(k):
        return (rep, f, lax.rem(t + k, NTP))

    own = []
    srcs = ((wq, wk, wv, wd), (wo,), (wg, wu), (wdn,))
    n = 0
    for g in range(4):
        at, copies = 0, []
        for src, width in zip(srcs[g], PARTS[g]):
            copies.append(pltpu.make_async_copy(src, bufs[g].at[z, y, :, at : at + width], lsem.at[n]))
            at += width
            n += 1
        for c in copies:
            c.start()
        own.append(copies)

    barrier = pltpu.get_barrier_semaphore()
    others = [*ynb, *znb, *(peer(k) for k in range(1, NTP))]
    for d in others:
        pl.semaphore_signal(barrier, inc=1, device_id=d, device_id_type=MESH)
    pl.semaphore_wait(barrier, len(others))

    base = (0, 16, 24, 32)

    def wrap_y(k):
        return lax.rem(y + k + NY, NY)

    def wrap_z(k):
        return lax.rem(z + k + NZ, NZ)

    def piece(g, kind, u, off):
        start, size = (A_ROWS if kind in (0, 2) else B_ROWS)[g][u]
        rows = slice(start, start + size)
        b = bufs[g]
        if kind == 0:
            return b.at[z, wrap_y(off), rows, :]
        if kind == 3:
            return b.at[:, wrap_y(off), rows, :]
        if kind == 1:
            return b.at[wrap_z(off), y, rows, :]
        return b.at[wrap_z(off), :, rows, :]

    def sem_of(kind, s, d, u):
        per = 8 if kind in (0, 3) else 4
        return base[kind] + d * per + s * 2 + u

    def message(g, kind, s, d, u, arriving):
        sign = -1 if d == 0 else 1
        ref = piece(g, kind, u, sign * (s + 1 if arriving else s))
        i = sem_of(kind, s, d, u)
        return pltpu.make_async_remote_copy(
            src_ref=ref,
            dst_ref=ref,
            send_sem=send.at[g, i],
            recv_sem=recv.at[g, i],
            device_id=(ynb if kind in (0, 3) else znb)[d],
            device_id_type=MESH,
        )

    started = []

    def start(g, kind, s, d, u):
        m = message(g, kind, s, d, u, False)
        m.start()
        started.append(m)

    def arrive(g, kind, s, d, u):
        message(g, kind, s, d, u, True).wait_recv()

    def last(kind):
        return 3 if kind in (0, 3) else 1

    def begin(g, kind):
        for u in (0, 1):
            for d in (0, 1):
                start(g, kind, 0, d, u)

    def step(g, kind, s):
        for u in (0, 1):
            for d in (0, 1):
                arrive(g, kind, s - 1, d, u)
                if s < last(kind) or u == d:
                    start(g, kind, s, d, u)

    def finish(g, kind):
        for d in (0, 1):
            arrive(g, kind, last(kind), d, d)

    def comm():
        def light(g):
            for c in own[g]:
                c.wait()
            begin(g, 0)
            begin(g, 1)
            yield
            step(g, 0, 1)
            step(g, 1, 1)
            yield
            step(g, 0, 2)
            yield
            step(g, 0, 3)
            finish(g, 1)
            yield
            finish(g, 0)

        def heavy(g):
            begin(g, 3)
            begin(g, 2)
            yield
            step(g, 3, 1)
            yield
            step(g, 3, 2)
            yield
            step(g, 2, 1)
            step(g, 3, 3)
            yield
            finish(g, 2)
            finish(g, 3)

        yield from light(0)
        for g in range(4):
            a, b = heavy(g), light(g + 1) if g < 3 else iter(())
            more = True
            while more:
                more = False
                for it in (a, b):
                    if next(it, "end") is None:
                        more = True
                        yield
            yield g

    stream = comm()
    done = [-1]

    def pump(n=1):
        for _ in range(n):
            r = next(stream, None)
            if r is not None:
                done[0] = r

    def until(g):
        while done[0] < g:
            pump()

    pump()

    def norm_rows(i, c):
        r = pl.ds(pl.multiple_of(i * 16, 16), 16)
        v = tok[r, :].astype(F32)
        xn[r, :] = (v * lax.rsqrt(jnp.mean(v * v, axis=-1, keepdims=True) + EPS) * gain1[...]).astype(BF16)
        return c

    lax.fori_loop(0, SEQ // 16, norm_rows, 0)
    pump()

    def build_mats(l, c):
        ti, si = iota((SEQ, 2 * SEQ), 0), lax.rem(iota((SEQ, 2 * SEQ), 1), SEQ)
        same = lax.shift_right_logical(ti, l) == lax.shift_right_logical(si, l)
        back = (ti - si) * (2 * (lax.shift_right_logical(ti, l) & 1) - 1)
        mats[2 * l] = jnp.where(same & (back >= 0), 1.0, 0.0).astype(BF16)
        mats[2 * l + 1] = jnp.where(same & (back > 0), 1.0, 0.0).astype(BF16)
        return c

    lax.fori_loop(0, LEVELS, build_mats, 0)
    until(0)
    pump(2)

    acc[...] = jnp.zeros_like(acc)

    def project(w, c):
        cols = pl.ds(pl.multiple_of(w * 512, 512), 512)
        acc[...] += dot(xn[:, cols], g1[w].reshape(512, 640))
        return c

    lax.fori_loop(0, NZ, project, 0)
    pump()
    gate = acc[:, 512:640] + bias[...]
    lane_head = lax.div(iota((SEQ, 128), 1), KW)
    extra = jnp.zeros((SEQ, 128), F32)
    for h in range(HEADS):
        extra = jnp.where(lane_head == h, spike[:, h : h + 1], extra)
    logs = (jnp.minimum(gate, 0.0) - jnp.log1p(jnp.exp(-jnp.abs(gate)))) / 16.0 + extra
    hi = logs.astype(BF16)
    decay2[0:SEQ, :] = hi
    decay2[SEQ : 2 * SEQ, :] = (logs - hi.astype(F32)).astype(BF16)
    qf[...] = acc[:, 0:128].astype(BF16).astype(F32)
    kf[...] = acc[:, 128:256].astype(BF16).astype(F32)
    vals = acc[:, 256:512]
    lane_vhead = lax.div(iota((SEQ, 256), 1), VW)
    for h in range(HEADS):
        vbd[h * SEQ : (h + 1) * SEQ, :] = jnp.where(lane_vhead == h, vals, 0.0).astype(BF16)

    def by_head(x):
        return jnp.concatenate([jnp.where(lane_head == h, x, 0.0).astype(BF16) for h in range(HEADS)], axis=0)

    score[...] = 2.0 * dot_t(qf[...].astype(BF16), by_head(kf[...]))
    pump()

    def level(l, c):
        left = (qf[...] * jnp.exp(dot(mats[2 * l], decay2[...]))).astype(BF16)
        right = by_head(kf[...] * jnp.exp(dot(mats[2 * l + 1], decay2[...])))
        differ = iota((SEQ, HEADS * SEQ), 0) ^ lax.rem(iota((SEQ, HEADS * SEQ), 1), SEQ)
        score[...] = jnp.where(differ >= lax.shift_left(1, l), dot_t(left, right), score[...])
        return c

    for lo, hi_ in ((0, 2), (2, 4), (4, 6), (6, 7)):
        lax.fori_loop(lo, hi_, level, 0)
        pump()
    mixed = dot(score[...].astype(BF16), vbd[...]) * (KW ** -0.5)
    sq = mixed * mixed
    sq_hi = sq.astype(BF16)
    sq_lo = (sq - sq_hi.astype(F32)).astype(BF16)
    ones = jnp.where(lax.div(iota((256, 256), 0), VW) == lax.div(iota((256, 256), 1), VW), 1.0, 0.0).astype(BF16)
    mean = (dot(sq_hi, ones) + dot(sq_lo, ones)) * (1.0 / VW)
    att[...] = (mixed * lax.rsqrt(mean + EPS) * hgain[...]).astype(BF16)
    until(1)
    pump(2)

    def project_out(left, weight, width, into):
        def body(w, c):
            cols = pl.ds(pl.multiple_of(w * 512, 512), 512)
            into[:, cols] = dot_t(left[...], weight[w].reshape(512, width)).astype(BF16)
            return c

        lax.fori_loop(0, NZ, body, 0)

    own_rows = pl.ds(pl.multiple_of(t * ROWS_OWN, ROWS_OWN), ROWS_OWN)

    def exchange(n, k, src, dst):
        return pltpu.make_async_remote_copy(
            src_ref=src, dst_ref=dst, send_sem=tsend.at[n, k], recv_sem=trecv.at[n, k],
            device_id=peer(k), device_id_type=MESH,
        )

    def scatter(n, src, dst):
        out_ = []
        for k in range(1, NTP):
            rows = pl.ds(pl.multiple_of(lax.rem(t + k, NTP) * ROWS_OWN, ROWS_OWN), ROWS_OWN)
            m = exchange(n, k, src.at[rows, :], dst.at[k])
            m.start()
            started.append(m)
            out_.append(m)
        return out_

    def spread(n, ref):
        for k in range(1, NTP):
            m = exchange(n, k, ref.at[own_rows, :], ref.at[own_rows, :])
            m.start()
            started.append(m)

    def spread_wait(n, ref):
        for k in range(1, NTP):
            rows = pl.ds(pl.multiple_of(lax.rem(t - k + NTP, NTP) * ROWS_OWN, ROWS_OWN), ROWS_OWN)
            exchange(n, k, ref.at[rows, :], ref.at[rows, :]).wait_recv()

    def total(src, dst):
        s = src[own_rows, :].astype(F32)
        for k in range(1, NTP):
            s = s + dst[k].astype(F32)
        return s

    project_out(att, g2, 256, part)
    moves = scatter(0, part, got)
    pump(2)
    for m in moves:
        m.wait_recv()
    residual = (tok[own_rows, :].astype(F32) + total(part, got)).astype(BF16).astype(F32)
    resid[...] = residual
    n2[own_rows, :] = (
        residual * lax.rsqrt(jnp.mean(residual * residual, axis=-1, keepdims=True) + EPS) * gain2[...]
    ).astype(BF16)
    spread(1, n2)
    pump(2)
    spread_wait(1, n2)
    until(2)
    pump(2)

    acc2[...] = jnp.zeros_like(acc2)

    def project2(w, c):
        cols = pl.ds(pl.multiple_of(w * 512, 512), 512)
        acc2[...] += dot(n2[:, cols], g3[w].reshape(512, 768))
        return c

    lax.fori_loop(0, NZ, project2, 0)
    pump()
    gated = acc2[:, 0:384]
    hid[...] = (gated / (1.0 + jnp.exp(-gated)) * acc2[:, 384:768]).astype(BF16)
    until(3)
    project_out(hid, g4, 384, part2)
    for m in scatter(2, part2, got2):
        m.wait_recv()
    out[own_rows, :] = (resid[...] + total(part2, got2)).astype(BF16)
    spread(3, out)
    spread_wait(3, out)
    for m in started:
        m.wait_send()


def shards(
    tokens, attention_norm_gain, query_weight, key_weight, value_weight, decay_weight, decay_gate_bias,
    decay_spike_extra, head_output_gain, output_weight, channel_norm_gain, gate_weight, up_weight, down_weight,
):
    vmem = pl.BlockSpec(memory_space=pltpu.VMEM)
    hbm = pl.BlockSpec(memory_space=pl.ANY)
    widths = [sum(p) for p in PARTS]
    return pl.pallas_call(
        layer_kernel,
        out_shape=jax.ShapeDtypeStruct((SEQ, D), BF16),
        in_specs=[vmem] * 6 + [hbm] * 8,
        out_specs=vmem,
        scratch_shapes=[
            *(pltpu.VMEM((NZ, NY, SLAB, w), BF16) for w in widths),
            pltpu.VMEM((SEQ, D), BF16),
            pltpu.VMEM((SEQ, 640), F32),
            pltpu.VMEM((2 * LEVELS, SEQ, 2 * SEQ), BF16),
            pltpu.VMEM((SEQ, HEADS * SEQ), F32),
            pltpu.VMEM((SEQ, 256), BF16),
            pltpu.VMEM((SEQ, D), BF16),
            pltpu.VMEM((NTP, ROWS_OWN, D), BF16),
            pltpu.VMEM((SEQ, D), BF16),
            pltpu.VMEM((SEQ, 768), F32),
            pltpu.VMEM((SEQ, 384), BF16),
            pltpu.VMEM((SEQ, D), BF16),
            pltpu.VMEM((NTP, ROWS_OWN, D), BF16),
            pltpu.VMEM((ROWS_OWN, D), F32),
            pltpu.VMEM((2 * SEQ, 128), BF16),
            pltpu.VMEM((SEQ, 128), F32),
            pltpu.VMEM((SEQ, 128), F32),
            pltpu.VMEM((HEADS * SEQ, 256), BF16),
            pltpu.SemaphoreType.DMA((8,)),
            pltpu.SemaphoreType.DMA((4, 48)),
            pltpu.SemaphoreType.DMA((4, 48)),
            pltpu.SemaphoreType.DMA((4, NTP)),
            pltpu.SemaphoreType.DMA((4, NTP)),
        ],
        compiler_params=pltpu.CompilerParams(collective_id=0, has_side_effects=True),
    )(
        tokens,
        attention_norm_gain.reshape(1, D),
        decay_gate_bias.reshape(1, 128),
        decay_spike_extra,
        jnp.tile(head_output_gain, HEADS).reshape(1, HEADS * VW),
        channel_norm_gain.reshape(1, D),
        query_weight, key_weight, value_weight, decay_weight, output_weight, gate_weight, up_weight, down_weight,
    )


def solution(mesh):
    rows, w = P(("rep", "fs"), None), P("fs", "tp")
    in_specs = (rows, P(), w, w, w, w, P("tp"), P(("rep", "fs"), "tp"), P(), w, P(), w, w, w)
    return jax.shard_map(shards, mesh=mesh, in_specs=in_specs, out_specs=rows, check_vma=False)
```

time: 345 us -> 124 us (0.36)
  waiting for transfers between devices: 242 us -> 0 us
  Pallas kernels: 0 us -> 120 us
  other arithmetic: 33 us -> 0 us
  local copies, waits for them, and re-layouts: 35.9 us -> 3.96 us
  matrix products: 18.3 us -> 0 us
  between operations: 13.4 us -> 0.01 us
    all_gather x3 -> x0, waiting for transfers between devices: 242 us -> none  [the longest x1 152 us: sent_together(): filled, at, outs = (lax.all_gather(both, axis, axis=dim, tiled=True), 0, [])]
    pallas_call x0 -> x1, Pallas kernels: none -> 120 us  [shards(): pl.pallas_call(layer_kernel, out_shape=jax.ShapeDtypeStruct((SEQ, D), BF1...]
    while x4 -> x0, local copies, waits for them, and re-layouts: 23.2 us -> none
    dot_general x19 -> x0, matrix products: 18.3 us -> none  [the longest x1 3.72 us: shards(): lax.dot_general(hidden, full_down, (((1,), (1,)), ((), ())), preferred_el...]
    exp x4 -> x0, other arithmetic: 12.3 us -> none  [advance(): jnp.exp(spread)]
    dot_general x4 -> x0, other arithmetic: 11.4 us -> none  [advance(): jnp.einsum('hid,hjd,hijd->hij', query_part, key_part, jnp.exp(spread), pr...]
    reduce_sum x5 -> x0, other arithmetic: 7.5 us -> none  [the longest x2 6 us: gathered_total(): return lax.all_gather(array, axis).astype(jnp.float32).sum(0)]
  transfers between devices with their start and end apart: 3 -> 0, of which waited for: 3 -> 0; matrix products, arithmetic and copies ran while one was open for 1% -> 0% of each run, Pallas kernels for 0% -> 0%
where the time goes in v1:
time: 124 us
  Pallas kernels  120 us (97%)
  local copies, waits for them, and re-layouts  3.96 us (3%)
    pallas_call x1, Pallas kernels, shards(): pl.pallas_call(layer_kernel, out_shape=jax.ShapeDtypeStruct((SEQ, D), BF1...  120 us
    unnamed x6, local copies, waits for them, and re-layouts  3.3 us

profile of v1, /device:TPU:1, one launch (start us, length us, event | category | flops | bytes accessed | tf_op | source)
XLA Modules:
  0.0 123.6 jit_solution(7485492770524479113)
XLA Ops:
  0.0 0.0 copy-start.1
  0.0 0.7 copy-done.1
  0.7 0.0 copy-start
  0.7 0.7 reshape_tile.3.hgain
  1.3 0.0 copy-done
  1.3 0.7 copy.15.spike
  2.1 119.7 %shard_map.136 = bf16[128,2048]{1,0:T(8,128)(2,1)} custom-call(bf16[128,2048]{1,0:T(8,128)(2,1)} %tok.1, f32[1,2048]{1,0:T(1,128)} %bitcast.3, f32[1,128]{1,0:T(1,128)} %bitcast.5, f32[128,4]{1,0:T(8,128)} %copy.15.spike, f32[1,256]{1,0:T(1,128)} %reshape_tile.3.hgain, f32[1,2048]{1,0:T(1,128)} %bitcast.4, bf16[64,128]{1,0:T(8,128)(2,1)} %wq.1, ...), custom_call_target="tpu_custom_call" | custom-call | tf_op jit(solution)/shard_map/pallas_call | solution.py:362
  121.7 1.9 %copy.17 = bf16[128,2048]{1,0:T(8,128)(2,1)} copy(bf16[128,2048]{1,0:T(8,128)(2,1)} %shard_map.136) | data formatting | bytes 1048576
  (1 shorter events, 0.0 us)
Async XLA Ops:
  0.0 0.7 copy-start.1
  0.7 0.7 copy-start

commit v2 on v1

v2 whole, which is shorter than its diff:
```python
import functools

import jax
import jax.numpy as jnp
from jax import lax
from jax.experimental import pallas as pl
from jax.experimental.pallas import tpu as pltpu
from jax.sharding import PartitionSpec as P

MESH = pl.DeviceIdType.MESH
F32, BF16 = jnp.float32, jnp.bfloat16
NY, NZ, NTP = 8, 4, 8
SEQ, D = 128, 2048
SLAB = D // (NY * NZ)
HEADS, KW, VW = 4, 32, 64
LEVELS = 7
EPS = 1e-6
PARTS = ((128, 128, 256, 128), (256,), (384, 384), (384,))
A_ROWS = (((0, 16), (16, 16)),) * 4
B_ROWS = (((32, 16), (48, 16)),) * 4
ROWS_OWN = SEQ // NTP


def link_plan(near, ahead, hop=2.6, rate=46.6e3, turn=6.5):
    units = (1, 1, 8, 4)
    cols = [sum(p) for p in PARTS]
    last = (3, 1, 1, 3)

    def rows(g, k, u):
        return (A_ROWS if k in (0, 2) else B_ROWS)[g][u][1]

    size = {
        (g, k, s, d, u): cols[g] * 2 * rows(g, k, u) * units[k]
        for g in range(4) for k in range(4) for s in range(last[k] + 1) for d in (0, 1) for u in (0, 1)
        if s < last[k] or u == d
    }

    def needs(m):
        g, k, s, d, u = m
        if s > 0:
            return {(g, k, s - 1, d, u)}
        if k < 2:
            return set()
        return {x for x in size if x[0] == g and x[1] == k - 2 and x[4] == u} if k == 2 else {
            x for x in size if x[0] == g and x[1] == 1 and x[4] == u
        }

    need = {m: needs(m) for m in size}
    then = {}
    for m, xs in need.items():
        for x in xs:
            then.setdefault(x, []).append(m)

    def urgency(m):
        g, k, s, d, u = m
        return (g * 10 - (ahead if k < 2 else 0), s, u, d)

    def link(m):
        return (m[1] in (0, 3), m[3])

    ready = {(a, d): [] for a in (True, False) for d in (0, 1)}
    free = dict.fromkeys(ready, 0.0)
    left = [sum(m[0] == g for m in size) for g in range(4)]
    for m in size:
        if not need[m]:
            ready[link(m)].append(m)
    now, ops, have, coming, at = 0.2, [], set(), [], 0
    while at < len(WORK) or coming:
        for l, queue in ready.items():
            while queue and free[l] - now < near:
                m = min(queue, key=urgency)
                queue.remove(m)
                free[l] = max(now, free[l]) + size[m] / rate
                coming.append((free[l] + hop, len(ops), m))
                ops.append(("send", m))
                now += 0.02
        coming.sort()
        if coming and coming[0][0] <= now:
            m = coming.pop(0)[2]
            ops.append(("take", m))
            now += 0.02
            if isinstance(m, str):
                have.add(m)
                continue
            left[m[0]] -= 1
            if left[m[0]] == 0:
                have.add(m[0])
            for x in then.get(m, ()):
                need[x].discard(m)
                if not need[x]:
                    ready[link(x)].append(x)
        elif at < len(WORK) and all(q in have for q in WORK[at][2]):
            name, span, _, gives = WORK[at]
            at += 1
            now += span
            ops.append(("work", name))
            if gives:
                coming.append((now + turn, len(ops), gives))
        else:
            now = max(now, min(coming)[0])
    return ops


WORK = (
    ("norm", 0.92, (), None),
    ("mats", 0.42, (), None),
    ("project", 1.1, (0,), None),
    ("prepare", 0.8, (), None),
    *((f"level{l}", 0.34, (), None) for l in range(LEVELS)),
    ("attend", 0.5, (), None),
    ("mix_out", 0.9, (1,), "scatter1"),
    ("residual", 0.3, ("scatter1",), "spread1"),
    ("gate_up", 1.1, ("spread1", 2), None),
    ("hidden", 0.2, (), None),
    ("down", 1.1, (3,), "scatter2"),
    ("layer_out", 0.3, ("scatter2",), "spread2"),
    ("end", 0.1, ("spread2",), None),
)
NEAR, AHEAD = 1.0, 12


def dot(a, b):
    return jnp.dot(a, b, preferred_element_type=F32)


def dot_t(a, b):
    return lax.dot_general(a, b, (((1,), (1,)), ((), ())), preferred_element_type=F32)


def iota(shape, axis):
    return lax.broadcasted_iota(jnp.int32, shape, axis)


def layer_kernel(
    tok_hbm, gain1, bias, spike, hgain, gain2, wq, wk, wv, wd, wo, wg, wu, wdn,
    out,
    tok, extra, fin,
    g1, g2, g3, g4, xn, acc, mats, score, att, part, got, n2, acc2, hid, part2, got2, resid, decay2, qf, kf, vbd,
    lsem, send, recv, tsend, trecv,
):
    bufs = (g1, g2, g3, g4)
    rep, f, t = lax.axis_index("rep"), lax.axis_index("fs"), lax.axis_index("tp")
    y, z = lax.rem(f, NY), lax.div(f, NY)
    zz = rep * NZ + z

    def at_y(k):
        return (rep, z * NY + lax.rem(y + k + NY, NY), t)

    def at_z(k):
        w = lax.rem(zz + k + 2 * NZ, 2 * NZ)
        return (lax.div(w, NZ), lax.rem(w, NZ) * NY + y, t)

    ynb, znb = (at_y(1), at_y(-1)), (at_z(1), at_z(-1))

    def peer(k):
        return (rep, f, lax.rem(t + k, NTP))

    barrier = pltpu.get_barrier_semaphore()
    others = [*ynb, *znb, *(peer(k) for k in range(1, NTP))]
    for d in others:
        pl.semaphore_signal(barrier, inc=1, device_id=d, device_id_type=MESH)

    own = []
    srcs = ((wq, wk, wv, wd), (wo,), (wg, wu), (wdn,))
    n = 0
    for g in range(4):
        at, copies = 0, []
        for src, width in zip(srcs[g], PARTS[g]):
            copies.append(pltpu.make_async_copy(src, bufs[g].at[z, y, :, at : at + width], lsem.at[n]))
            at += width
            n += 1
        for c in copies:
            c.start()
        own.append(copies)
        if g == 0:
            tok_copy = pltpu.make_async_copy(tok_hbm, tok, lsem.at[8])
            tok_copy.start()

    pl.semaphore_wait(barrier, len(others))

    base = (0, 16, 24, 32)

    def wrap_y(k):
        return lax.rem(y + k + NY, NY)

    def wrap_z(k):
        return lax.rem(z + k + NZ, NZ)

    def piece(g, kind, u, off):
        start, size = (A_ROWS if kind in (0, 2) else B_ROWS)[g][u]
        rows = slice(start, start + size)
        b = bufs[g]
        if kind == 0:
            return b.at[z, wrap_y(off), rows, :]
        if kind == 3:
            return b.at[:, wrap_y(off), rows, :]
        if kind == 1:
            return b.at[wrap_z(off), y, rows, :]
        return b.at[wrap_z(off), :, rows, :]

    def sem_of(kind, s, d, u):
        per = 8 if kind in (0, 3) else 4
        return base[kind] + d * per + s * 2 + u

    def message(g, kind, s, d, u, arriving):
        sign = -1 if d == 0 else 1
        ref = piece(g, kind, u, sign * (s + 1 if arriving else s))
        i = sem_of(kind, s, d, u)
        return pltpu.make_async_remote_copy(
            src_ref=ref,
            dst_ref=ref,
            send_sem=send.at[g, i],
            recv_sem=recv.at[g, i],
            device_id=(ynb if kind in (0, 3) else znb)[d],
            device_id_type=MESH,
        )

    started = []

    def start(g, kind, s, d, u):
        m = message(g, kind, s, d, u, False)
        m.start()
        started.append(m)

    def arrive(g, kind, s, d, u):
        message(g, kind, s, d, u, True).wait_recv()

    def norm_rows(i, c):
        r = pl.ds(pl.multiple_of(i * 16, 16), 16)
        v = tok[r, :].astype(F32)
        xn[r, :] = (v * lax.rsqrt(jnp.mean(v * v, axis=-1, keepdims=True) + EPS) * gain1[...]).astype(BF16)
        return c

    def norm():
        tok_copy.wait()
        lax.fori_loop(0, SEQ // 16, norm_rows, 0)

    def build_mats(l, c):
        ti, si = iota((SEQ, 2 * SEQ), 0), lax.rem(iota((SEQ, 2 * SEQ), 1), SEQ)
        same = lax.shift_right_logical(ti, l) == lax.shift_right_logical(si, l)
        back = (ti - si) * (2 * (lax.shift_right_logical(ti, l) & 1) - 1)
        mats[2 * l] = jnp.where(same & (back >= 0), 1.0, 0.0).astype(BF16)
        mats[2 * l + 1] = jnp.where(same & (back > 0), 1.0, 0.0).astype(BF16)
        return c

    def build():
        lax.fori_loop(0, LEVELS, build_mats, 0)
        heads = jnp.where(lax.div(iota((HEADS, 128), 1), KW) == iota((HEADS, 128), 0), 1.0, 0.0)
        extra[...] = lax.dot_general(
            spike[...], heads, (((0,), (0,)), ((), ())), precision=lax.Precision.HIGHEST, preferred_element_type=F32
        )

    def project():
        acc[...] = jnp.zeros_like(acc)

        def body(w, c):
            cols = pl.ds(pl.multiple_of(w * 512, 512), 512)
            acc[...] += dot(xn[:, cols], g1[w].reshape(512, 640))
            return c

        lax.fori_loop(0, NZ, body, 0)

    lane_head = lax.div(iota((SEQ, 128), 1), KW)

    def by_head(x):
        return jnp.concatenate([jnp.where(lane_head == h, x, 0.0).astype(BF16) for h in range(HEADS)], axis=0)

    def prepare():
        gate = acc[:, 512:640] + bias[...]
        logs = (jnp.minimum(gate, 0.0) - jnp.log1p(jnp.exp(-jnp.abs(gate)))) / 16.0 + extra[...]
        hi = logs.astype(BF16)
        decay2[0:SEQ, :] = hi
        decay2[SEQ : 2 * SEQ, :] = (logs - hi.astype(F32)).astype(BF16)
        qf[...] = acc[:, 0:128].astype(BF16).astype(F32)
        kf[...] = acc[:, 128:256].astype(BF16).astype(F32)
        vals = acc[:, 256:512]
        lane_vhead = lax.div(iota((SEQ, 256), 1), VW)
        for h in range(HEADS):
            vbd[h * SEQ : (h + 1) * SEQ, :] = jnp.where(lane_vhead == h, vals, 0.0).astype(BF16)
        score[...] = 2.0 * dot_t(qf[...].astype(BF16), by_head(kf[...]))

    def level(l):
        left = (qf[...] * jnp.exp(dot(mats[2 * l], decay2[...]))).astype(BF16)
        right = by_head(kf[...] * jnp.exp(dot(mats[2 * l + 1], decay2[...])))
        differ = iota((SEQ, HEADS * SEQ), 0) ^ lax.rem(iota((SEQ, HEADS * SEQ), 1), SEQ)
        score[...] = jnp.where(differ >= 2 ** l, dot_t(left, right), score[...])

    def attend():
        mixed = dot(score[...].astype(BF16), vbd[...]) * (KW ** -0.5)
        sq = mixed * mixed
        sq_hi = sq.astype(BF16)
        sq_lo = (sq - sq_hi.astype(F32)).astype(BF16)
        ones = jnp.where(lax.div(iota((256, 256), 0), VW) == lax.div(iota((256, 256), 1), VW), 1.0, 0.0).astype(BF16)
        mean = (dot(sq_hi, ones) + dot(sq_lo, ones)) * (1.0 / VW)
        gains = jnp.concatenate([hgain[...]] * HEADS, axis=1)
        att[...] = (mixed * lax.rsqrt(mean + EPS) * gains).astype(BF16)

    def project_out(left, weight, width, into):
        def body(w, c):
            cols = pl.ds(pl.multiple_of(w * 512, 512), 512)
            into[:, cols] = dot_t(left[...], weight[w].reshape(512, width)).astype(BF16)
            return c

        lax.fori_loop(0, NZ, body, 0)

    def rows_of(k):
        return pl.ds(pl.multiple_of(lax.rem(t + k + NTP, NTP) * ROWS_OWN, ROWS_OWN), ROWS_OWN)

    own_rows = rows_of(0)

    def exchange(n, k, src, dst):
        return pltpu.make_async_remote_copy(
            src_ref=src, dst_ref=dst, send_sem=tsend.at[n, k], recv_sem=trecv.at[n, k],
            device_id=peer(k), device_id_type=MESH,
        )

    def go(copy):
        copy.start()
        started.append(copy)

    def scatter(n, src, dst):
        for k in range(1, NTP):
            go(exchange(n, k, src.at[rows_of(k), :], dst.at[k]))

    def scatter_wait(n, src, dst):
        for k in range(1, NTP):
            exchange(n, k, src.at[rows_of(k), :], dst.at[k]).wait_recv()

    def spread(n, src, ref):
        for k in range(1, NTP):
            go(exchange(n, k, src, ref.at[own_rows, :]))

    def spread_wait(n, src, ref):
        for k in range(1, NTP):
            exchange(n, k, src, ref.at[rows_of(-k), :]).wait_recv()

    def total(src, dst):
        s = src[own_rows, :].astype(F32)
        for k in range(1, NTP):
            s = s + dst[k].astype(F32)
        return s

    def mix_out():
        project_out(att, g2, 256, part)
        scatter(0, part, got)

    def residual_rows():
        r = (tok[own_rows, :].astype(F32) + total(part, got)).astype(BF16).astype(F32)
        resid[...] = r
        n2[own_rows, :] = (r * lax.rsqrt(jnp.mean(r * r, axis=-1, keepdims=True) + EPS) * gain2[...]).astype(BF16)
        spread(1, n2.at[own_rows, :], n2)

    def gate_up():
        acc2[...] = jnp.zeros_like(acc2)

        def body(w, c):
            cols = pl.ds(pl.multiple_of(w * 512, 512), 512)
            acc2[...] += dot(n2[:, cols], g3[w].reshape(512, 768))
            return c

        lax.fori_loop(0, NZ, body, 0)

    def hidden():
        gated = acc2[:, 0:384]
        hid[...] = (gated / (1.0 + jnp.exp(-gated)) * acc2[:, 384:768]).astype(BF16)

    def down():
        project_out(hid, g4, 384, part2)
        scatter(2, part2, got2)

    own_out = pltpu.make_async_copy(fin, out.at[own_rows, :], lsem.at[9])

    def layer_out():
        fin[...] = (resid[...] + total(part2, got2)).astype(BF16)
        spread(3, fin, out)
        own_out.start()

    def end():
        own_out.wait()

    work = dict(
        norm=norm, mats=build, project=project, prepare=prepare, attend=attend, mix_out=mix_out,
        residual=residual_rows, gate_up=gate_up, hidden=hidden, down=down, layer_out=layer_out, end=end,
        **{f"level{l}": functools.partial(level, l) for l in range(LEVELS)},
    )
    waits = dict(
        scatter1=lambda: scatter_wait(0, part, got), spread1=lambda: spread_wait(1, n2.at[own_rows, :], n2),
        scatter2=lambda: scatter_wait(2, part2, got2), spread2=lambda: spread_wait(3, fin, out),
    )
    waiting = set(range(4))
    for verb, what in link_plan(NEAR, AHEAD):
        with jax.named_scope(f"{verb}_{what}".replace(" ", "")):
            if verb == "work":
                work[what]()
            elif verb == "send":
                if what[0] in waiting:
                    waiting.discard(what[0])
                    for c in own[what[0]]:
                        c.wait()
                start(*what)
            elif isinstance(what, str):
                waits[what]()
            else:
                arrive(*what)
    for m in started:
        m.wait_send()


def shards(
    tokens, attention_norm_gain, query_weight, key_weight, value_weight, decay_weight, decay_gate_bias,
    decay_spike_extra, head_output_gain, output_weight, channel_norm_gain, gate_weight, up_weight, down_weight,
):
    vmem = pl.BlockSpec(memory_space=pltpu.VMEM)
    hbm = pl.BlockSpec(memory_space=pl.ANY)
    widths = [sum(p) for p in PARTS]
    return pl.pallas_call(
        layer_kernel,
        out_shape=jax.ShapeDtypeStruct((SEQ, D), BF16),
        in_specs=[hbm] + [vmem] * 5 + [hbm] * 8,
        out_specs=hbm,
        scratch_shapes=[
            pltpu.VMEM((SEQ, D), BF16),
            pltpu.VMEM((SEQ, 128), F32),
            pltpu.VMEM((ROWS_OWN, D), BF16),
            *(pltpu.VMEM((NZ, NY, SLAB, w), BF16) for w in widths),
            pltpu.VMEM((SEQ, D), BF16),
            pltpu.VMEM((SEQ, 640), F32),
            pltpu.VMEM((2 * LEVELS, SEQ, 2 * SEQ), BF16),
            pltpu.VMEM((SEQ, HEADS * SEQ), F32),
            pltpu.VMEM((SEQ, 256), BF16),
            pltpu.VMEM((SEQ, D), BF16),
            pltpu.VMEM((NTP, ROWS_OWN, D), BF16),
            pltpu.VMEM((SEQ, D), BF16),
            pltpu.VMEM((SEQ, 768), F32),
            pltpu.VMEM((SEQ, 384), BF16),
            pltpu.VMEM((SEQ, D), BF16),
            pltpu.VMEM((NTP, ROWS_OWN, D), BF16),
            pltpu.VMEM((ROWS_OWN, D), F32),
            pltpu.VMEM((2 * SEQ, 128), BF16),
            pltpu.VMEM((SEQ, 128), F32),
            pltpu.VMEM((SEQ, 128), F32),
            pltpu.VMEM((HEADS * SEQ, 256), BF16),
            pltpu.SemaphoreType.DMA((10,)),
            pltpu.SemaphoreType.DMA((4, 48)),
            pltpu.SemaphoreType.DMA((4, 48)),
            pltpu.SemaphoreType.DMA((4, NTP)),
            pltpu.SemaphoreType.DMA((4, NTP)),
        ],
        compiler_params=pltpu.CompilerParams(collective_id=0, has_side_effects=True),
    )(
        tokens,
        attention_norm_gain.reshape(1, D),
        decay_gate_bias.reshape(1, 128),
        decay_spike_extra.T,
        head_output_gain.reshape(1, VW),
        channel_norm_gain.reshape(1, D),
        query_weight, key_weight, value_weight, decay_weight, output_weight, gate_weight, up_weight, down_weight,
    )


def solution(mesh):
    rows, w = P(("rep", "fs"), None), P("fs", "tp")
    in_specs = (rows, P(), w, w, w, w, P("tp"), P(("rep", "fs"), "tp"), P(), w, P(), w, w, w)
    return jax.shard_map(shards, mesh=mesh, in_specs=in_specs, out_specs=rows, check_vma=False)
```

time: 124 us -> 94.2 us (0.76)
  Pallas kernels: 120 us -> 92.1 us
  local copies, waits for them, and re-layouts: 3.96 us -> 1.88 us
    pallas_call x1, Pallas kernels: 120 us -> 92.1 us  [shards(): pl.pallas_call(layer_kernel, out_shape=jax.ShapeDtypeStruct((SEQ, D), BF1...]
    unnamed x6 -> x1, local copies, waits for them, and re-layouts: 3.3 us -> 1.88 us
where the time goes in v2:
time: 94.2 us; the launch traced here: 94 us
  Pallas kernels  92.1 us (98%)
  local copies, waits for them, and re-layouts  1.88 us (2%)
    pallas_call x1, Pallas kernels, shards(): pl.pallas_call(layer_kernel, out_shape=jax.ShapeDtypeStruct((SEQ, D), BF1...  92.1 us

profile of v2, /device:TPU:1, one launch (start us, length us, event | category | flops | bytes accessed | tf_op | source)
XLA Modules:
  0.0 94.0 jit_solution(9682525922270059877)
XLA Ops:
  0.0 92.1 %shard_map.136 = bf16[128,2048]{1,0:T(8,128)(2,1)} custom-call(bf16[128,2048]{1,0:T(8,128)(2,1)} %tok_hbm.1, f32[1,2048]{1,0:T(1,128)} %bitcast.5, f32[1,128]{1,0:T(1,128)} %bitcast.8, f32[4,128]{1,0:T(4,128)} %bitcast.7, f32[1,64]{1,0:T(1,128)} %bitcast.9, f32[1,2048]{1,0:T(1,128)} %bitcast.6, bf16[64,128]{1,0:T(8,128)(2,1)} %wq.1, bf16[64,128]{1,0:T(8,128)(2,1)} %wk.1, ...), custom_call_target="tpu_custom_call" | custom-call | tf_op jit(solution)/shard_map/pallas_call | solution.py:416
  92.1 1.9 %copy.16 = bf16[128,2048]{1,0:T(8,128)(2,1)} copy(bf16[128,2048]{1,0:T(8,128)(2,1)} %shard_map.136) | data formatting | bytes 1048576

commit v3 on v2

--- a/solution.py
+++ b/solution.py
@@ -16,64 +16,87 @@
 LEVELS = 7
 EPS = 1e-6
 PARTS = ((128, 128, 256, 128), (256,), (384, 384), (384,))
-A_ROWS = (((0, 16), (16, 16)),) * 4
-B_ROWS = (((32, 16), (48, 16)),) * 4
+A_ROWS = (32, 32, 32, 48)
 ROWS_OWN = SEQ // NTP
 
 
-def link_plan(near, ahead, hop=2.6, rate=46.6e3, turn=6.5):
-    units = (1, 1, 8, 4)
-    cols = [sum(p) for p in PARTS]
-    last = (3, 1, 1, 3)
-
-    def rows(g, k, u):
-        return (A_ROWS if k in (0, 2) else B_ROWS)[g][u][1]
-
-    size = {
-        (g, k, s, d, u): cols[g] * 2 * rows(g, k, u) * units[k]
-        for g in range(4) for k in range(4) for s in range(last[k] + 1) for d in (0, 1) for u in (0, 1)
-        if s < last[k] or u == d
-    }
-
-    def needs(m):
-        g, k, s, d, u = m
-        if s > 0:
-            return {(g, k, s - 1, d, u)}
-        if k < 2:
-            return set()
-        return {x for x in size if x[0] == g and x[1] == k - 2 and x[4] == u} if k == 2 else {
-            x for x in size if x[0] == g and x[1] == 1 and x[4] == u
-        }
-
-    need = {m: needs(m) for m in size}
-    then = {}
-    for m, xs in need.items():
-        for x in xs:
+def messages(g):
+    ra = A_ROWS[g]
+    rows_a, rows_b = slice(0, ra), slice(ra, SLAB)
+    half_a = (slice(0, 16 * ((ra // 16 + 1) // 2)), slice(16 * ((ra // 16 + 1) // 2), ra))
+    half_b = (slice(ra, ra + 16 * ((SLAB - ra) // 32)), slice(ra + 16 * ((SLAB - ra) // 32), SLAB))
+    out = {}
+    for d in (0, 1):
+        back = -1 if d == 0 else 1
+        for s in range(4):
+            out["ay", d, s] = ("y", 0, back * s, rows_a if s < 3 else half_a[d], (("ay", s - 1),) if s else (), ("ay", s))
+        for i, off in enumerate((0, -1, 1, -2, 2, -3, 3, 4)):
+            out["az", d, i] = ("z", 0, off, rows_a, (("ay", (i - 1) // 2),) if i else (), ("az", 0))
+        out["az", d, 8] = ("z", back, slice(4 * d, 4 * d + 4), rows_a, (("az", 0),), ("az", 1))
+        out["bz", d, 0] = ("z", 0, 0, rows_b, (), ("bz", 0))
+        if half_b[d].stop > half_b[d].start:
+            out["bz", d, 1] = ("z", back, 0, half_b[d], (("bz", 0),), ("bz", 1))
+        for i, off in enumerate((0, -1, 1, 2)):
+            out["by", d, i] = ("y", off, 0, rows_b, (("bz", i // 3),) if i else (), ("by", 0))
+        for s in (1, 2):
+            for h in (0, 1):
+                half = slice(2 * h, 2 * h + 2)
+                out["by", d, 2 + 2 * s + h] = (
+                    "y", half, back * s, rows_b, (("by", 2 * s - 3 + h if s > 1 else 0),), ("by", 2 * s - 1 + h),
+                )
+        out["by", d, 8] = ("y", slice(2 * d, 2 * d + 2), back * 3, rows_b, (("by", 3 + d),), ("by", 5))
+    return out
+
+
+TAKES = [("ay", 0), ("ay", 1), ("ay", 2), ("ay", 3), ("az", 0), ("az", 1), ("bz", 0), ("bz", 1), *(("by", i) for i in range(6))]
+
+
+def extent(i):
+    return i.stop - i.start if isinstance(i, slice) else 1
+
+
+def link_plan(near, ahead, hop=2.6, rate=46.6e3, turn=7.5, times=None):
+    table = {(g, *m): v for g in range(4) for m, v in messages(g).items()}
+    need = {m: {(m[0], *x) for x in v[4]} for m, v in table.items()}
+    feeds, then = {}, {}
+    for m, v in table.items():
+        feeds.setdefault((m[0], *v[5]), set()).add(m)
+        for x in need[m]:
             then.setdefault(x, []).append(m)
 
     def urgency(m):
-        g, k, s, d, u = m
-        return (g * 10 - (ahead if k < 2 else 0), s, u, d)
-
-    def link(m):
-        return (m[1] in (0, 3), m[3])
-
-    ready = {(a, d): [] for a in (True, False) for d in (0, 1)}
+        g, name, d, i = m
+        second = name == "by" or name == "az"
+        return (g * 10 - (0 if second else ahead), i, d)
+
+    ready = {(a, d): [] for a in ("y", "z") for d in (0, 1)}
     free = dict.fromkeys(ready, 0.0)
-    left = [sum(m[0] == g for m in size) for g in range(4)]
-    for m in size:
+    left = [sum(x[0] == g for x in feeds) for g in range(4)]
+    for m, v in table.items():
         if not need[m]:
-            ready[link(m)].append(m)
+            ready[v[0], m[2]].append(m)
     now, ops, have, coming, at = 0.2, [], set(), [], 0
-    while at < len(WORK) or coming:
+    landed = {}
+    def fill(until):
+        nonlocal now
+        before = len(ops)
         for l, queue in ready.items():
-            while queue and free[l] - now < near:
+            while queue and free[l] < until:
                 m = min(queue, key=urgency)
                 queue.remove(m)
-                free[l] = max(now, free[l]) + size[m] / rate
-                coming.append((free[l] + hop, len(ops), m))
+                v = table[m]
+                size = extent(v[1]) * extent(v[2]) * extent(v[3]) * sum(PARTS[m[0]]) * 2
+                free[l] = max(now, free[l]) + size / rate
+                landed[m] = free[l] + hop
+                take = (m[0], *v[5])
+                if all(x in landed for x in feeds[take]):
+                    coming.append((max(landed[x] for x in feeds[take]), len(ops), take))
                 ops.append(("send", m))
                 now += 0.02
+        return len(ops) > before
+
+    while at < len(WORK) or coming:
+        fill(now + near)
         coming.sort()
         if coming and coming[0][0] <= now:
             m = coming.pop(0)[2]
@@ -85,19 +108,24 @@
             left[m[0]] -= 1
             if left[m[0]] == 0:
                 have.add(m[0])
+                if times is not None:
+                    times[m[0]] = now
             for x in then.get(m, ()):
                 need[x].discard(m)
                 if not need[x]:
-                    ready[link(x)].append(x)
+                    ready[table[x][0], x[2]].append(x)
         elif at < len(WORK) and all(q in have for q in WORK[at][2]):
             name, span, _, gives = WORK[at]
             at += 1
+            fill(now + span)
             now += span
             ops.append(("work", name))
             if gives:
                 coming.append((now + turn, len(ops), gives))
-        else:
+        elif not fill(min(coming)[0] if coming else now + 1e3):
             now = max(now, min(coming)[0])
+    if times is not None:
+        times["end"] = now
     return ops
 
 
@@ -105,7 +133,7 @@
     ("norm", 0.92, (), None),
     ("mats", 0.42, (), None),
     ("project", 1.1, (0,), None),
-    ("prepare", 0.8, (), None),
+    ("prepare", 0.27, (), None),
     *((f"level{l}", 0.34, (), None) for l in range(LEVELS)),
     ("attend", 0.5, (), None),
     ("mix_out", 0.9, (1,), "scatter1"),
@@ -116,7 +144,7 @@
     ("layer_out", 0.3, ("scatter2",), "spread2"),
     ("end", 0.1, ("spread2",), None),
 )
-NEAR, AHEAD = 1.0, 12
+NEAR, AHEAD = 0.5, 12
 
 
 def dot(a, b):
@@ -162,68 +190,48 @@
 
     own = []
     srcs = ((wq, wk, wv, wd), (wo,), (wg, wu), (wdn,))
-    n = 0
     for g in range(4):
         at, copies = 0, []
         for src, width in zip(srcs[g], PARTS[g]):
-            copies.append(pltpu.make_async_copy(src, bufs[g].at[z, y, :, at : at + width], lsem.at[n]))
+            copies.append(pltpu.make_async_copy(src, bufs[g].at[z, y, :, at : at + width], lsem.at[g]))
             at += width
-            n += 1
         for c in copies:
             c.start()
-        own.append(copies)
+        own.append(pltpu.make_async_copy(bufs[g].at[z, y], bufs[g].at[z, y], lsem.at[g]))
         if g == 0:
-            tok_copy = pltpu.make_async_copy(tok_hbm, tok, lsem.at[8])
+            tok_copy = pltpu.make_async_copy(tok_hbm, tok, lsem.at[4])
             tok_copy.start()
 
     pl.semaphore_wait(barrier, len(others))
 
-    base = (0, 16, 24, 32)
-
-    def wrap_y(k):
-        return lax.rem(y + k + NY, NY)
-
-    def wrap_z(k):
-        return lax.rem(z + k + NZ, NZ)
-
-    def piece(g, kind, u, off):
-        start, size = (A_ROWS if kind in (0, 2) else B_ROWS)[g][u]
-        rows = slice(start, start + size)
-        b = bufs[g]
-        if kind == 0:
-            return b.at[z, wrap_y(off), rows, :]
-        if kind == 3:
-            return b.at[:, wrap_y(off), rows, :]
-        if kind == 1:
-            return b.at[wrap_z(off), y, rows, :]
-        return b.at[wrap_z(off), :, rows, :]
-
-    def sem_of(kind, s, d, u):
-        per = 8 if kind in (0, 3) else 4
-        return base[kind] + d * per + s * 2 + u
-
-    def message(g, kind, s, d, u, arriving):
-        sign = -1 if d == 0 else 1
-        ref = piece(g, kind, u, sign * (s + 1 if arriving else s))
-        i = sem_of(kind, s, d, u)
-        return pltpu.make_async_remote_copy(
-            src_ref=ref,
-            dst_ref=ref,
-            send_sem=send.at[g, i],
-            recv_sem=recv.at[g, i],
-            device_id=(ynb if kind in (0, 3) else znb)[d],
-            device_id_type=MESH,
-        )
-
-    started = []
-
-    def start(g, kind, s, d, u):
-        m = message(g, kind, s, d, u, False)
-        m.start()
-        started.append(m)
-
-    def arrive(g, kind, s, d, u):
-        message(g, kind, s, d, u, True).wait_recv()
+    tables = [messages(g) for g in range(4)]
+
+    def place(i, at, n):
+        return i if isinstance(i, slice) else lax.rem(at + i + n, n)
+
+    def send_weight(g, name, d, i):
+        ring, zs, ys, rows, _, take = tables[g][name, d, i]
+        ref = bufs[g].at[place(zs, z, NZ), place(ys, y, NY), rows, :]
+        pltpu.make_async_remote_copy(
+            src_ref=ref, dst_ref=ref, send_sem=send.at[g], recv_sem=recv.at[g, TAKES.index(take)],
+            device_id=(ynb if ring == "y" else znb)[d], device_id_type=MESH,
+        ).start()
+
+    def wait_bytes(ref, sem):
+        pltpu.make_async_copy(ref, ref, sem).wait()
+
+    def take_weight(g, name, i):
+        slabs, rows = 0, None
+        for v in tables[g].values():
+            if v[5] == (name, i):
+                whole = extent(v[3])
+                slabs += extent(v[1]) * extent(v[2]) * whole
+        for nz, ny, size in ((1, 1, SLAB), (1, 2, SLAB), (1, 4, SLAB), (1, 8, SLAB), (2, 8, SLAB), (3, 8, SLAB)):
+            if slabs % (nz * ny * 16) == 0 and slabs <= nz * ny * size:
+                ref = bufs[g].at[0:nz, 0:ny, 0 : slabs // (nz * ny), :]
+                wait_bytes(ref, recv.at[g, TAKES.index((name, i))])
+                return
+        raise ValueError(name)
 
     def norm_rows(i, c):
         r = pl.ds(pl.multiple_of(i * 16, 16), 16)
@@ -309,30 +317,21 @@
     own_rows = rows_of(0)
 
     def exchange(n, k, src, dst):
-        return pltpu.make_async_remote_copy(
-            src_ref=src, dst_ref=dst, send_sem=tsend.at[n, k], recv_sem=trecv.at[n, k],
+        pltpu.make_async_remote_copy(
+            src_ref=src, dst_ref=dst, send_sem=tsend.at[n], recv_sem=trecv.at[n],
             device_id=peer(k), device_id_type=MESH,
-        )
-
-    def go(copy):
-        copy.start()
-        started.append(copy)
+        ).start()
 
     def scatter(n, src, dst):
         for k in range(1, NTP):
-            go(exchange(n, k, src.at[rows_of(k), :], dst.at[k]))
-
-    def scatter_wait(n, src, dst):
-        for k in range(1, NTP):
-            exchange(n, k, src.at[rows_of(k), :], dst.at[k]).wait_recv()
+            exchange(n, k, src.at[rows_of(k), :], dst.at[k])
 
     def spread(n, src, ref):
         for k in range(1, NTP):
-            go(exchange(n, k, src, ref.at[own_rows, :]))
-
-    def spread_wait(n, src, ref):
-        for k in range(1, NTP):
-            exchange(n, k, src, ref.at[rows_of(-k), :]).wait_recv()
+            exchange(n, k, src, ref.at[own_rows, :])
+
+    def exchange_wait(n, sem):
+        wait_bytes(part.at[0 : SEQ - ROWS_OWN, :], sem.at[n])
 
     def total(src, dst):
         s = src[own_rows, :].astype(F32)
@@ -368,7 +367,7 @@
         project_out(hid, g4, 384, part2)
         scatter(2, part2, got2)
 
-    own_out = pltpu.make_async_copy(fin, out.at[own_rows, :], lsem.at[9])
+    own_out = pltpu.make_async_copy(fin, out.at[own_rows, :], lsem.at[5])
 
     def layer_out():
         fin[...] = (resid[...] + total(part2, got2)).astype(BF16)
@@ -383,10 +382,7 @@
         residual=residual_rows, gate_up=gate_up, hidden=hidden, down=down, layer_out=layer_out, end=end,
         **{f"level{l}": functools.partial(level, l) for l in range(LEVELS)},
     )
-    waits = dict(
-        scatter1=lambda: scatter_wait(0, part, got), spread1=lambda: spread_wait(1, n2.at[own_rows, :], n2),
-        scatter2=lambda: scatter_wait(2, part2, got2), spread2=lambda: spread_wait(3, fin, out),
-    )
+    turns = dict(scatter1=0, spread1=1, scatter2=2, spread2=3)
     waiting = set(range(4))
     for verb, what in link_plan(NEAR, AHEAD):
         with jax.named_scope(f"{verb}_{what}".replace(" ", "")):
@@ -395,15 +391,16 @@
             elif verb == "send":
                 if what[0] in waiting:
                     waiting.discard(what[0])
-                    for c in own[what[0]]:
-                        c.wait()
-                start(*what)
+                    own[what[0]].wait()
+                send_weight(*what)
             elif isinstance(what, str):
-                waits[what]()
+                exchange_wait(turns[what], trecv)
             else:
-                arrive(*what)
-    for m in started:
-        m.wait_send()
+                take_weight(*what)
+    for g in range(4):
+        wait_bytes(bufs[g].at[0:3], send.at[g])
+        wait_bytes(bufs[g].at[3, 0:7], send.at[g])
+        exchange_wait(g, tsend)
 
 
 def shards(
@@ -440,11 +437,11 @@
             pltpu.VMEM((SEQ, 128), F32),
             pltpu.VMEM((SEQ, 128), F32),
             pltpu.VMEM((HEADS * SEQ, 256), BF16),
-            pltpu.SemaphoreType.DMA((10,)),
-            pltpu.SemaphoreType.DMA((4, 48)),
-            pltpu.SemaphoreType.DMA((4, 48)),
-            pltpu.SemaphoreType.DMA((4, NTP)),
-            pltpu.SemaphoreType.DMA((4, NTP)),
+            pltpu.SemaphoreType.DMA((6,)),
+            pltpu.SemaphoreType.DMA((4,)),
+            pltpu.SemaphoreType.DMA((4, len(TAKES))),
+            pltpu.SemaphoreType.DMA((4,)),
+            pltpu.SemaphoreType.DMA((4,)),
         ],
         compiler_params=pltpu.CompilerParams(collective_id=0, has_side_effects=True),
     )(

time: 94.2 us -> 86.5 us (0.918)
  Pallas kernels: 92.1 us -> 84.4 us
    pallas_call x1, Pallas kernels: 92.1 us -> 84.4 us  [shards(): pl.pallas_call(layer_kernel, out_shape=jax.ShapeDtypeStruct((SEQ, D), BF1...]
where the time goes in v3:
time: 86.5 us; the launch traced here: 86.3 us
  Pallas kernels  84.4 us (98%)
  local copies, waits for them, and re-layouts  1.88 us (2%)
    pallas_call x1, Pallas kernels, shards(): pl.pallas_call(layer_kernel, out_shape=jax.ShapeDtypeStruct((SEQ, D), BF1...  84.4 us
    unnamed x1, local copies, waits for them, and re-layouts  1.88 us

profile of v3, /device:TPU:1, one launch (start us, length us, event | category | flops | bytes accessed | tf_op | source)
XLA Modules:
  0.0 86.3 jit_solution(6926593404067816061)
XLA Ops:
  0.0 84.4 %shard_map.136 = bf16[128,2048]{1,0:T(8,128)(2,1)} custom-call(bf16[128,2048]{1,0:T(8,128)(2,1)} %tok_hbm.1, f32[1,2048]{1,0:T(1,128)} %bitcast.5, f32[1,128]{1,0:T(1,128)} %bitcast.8, f32[4,128]{1,0:T(4,128)} %bitcast.7, f32[1,64]{1,0:T(1,128)} %bitcast.9, f32[1,2048]{1,0:T(1,128)} %bitcast.6, bf16[64,128]{1,0:T(8,128)(2,1)} %wq.1, bf16[64,128]{1,0:T(8,128)(2,1)} %wk.1, ...), custom_call_target="tpu_custom_call" | custom-call | tf_op jit(solution)/shard_map/pallas_call | solution.py:413
  84.4 1.9 %copy.16 = bf16[128,2048]{1,0:T(8,128)(2,1)} copy(bf16[128,2048]{1,0:T(8,128)(2,1)} %shard_map.136) | data formatting | bytes 1048576

commit v4 on v3

--- a/solution.py
+++ b/solution.py
@@ -16,7 +16,7 @@
 LEVELS = 7
 EPS = 1e-6
 PARTS = ((128, 128, 256, 128), (256,), (384, 384), (384,))
-A_ROWS = (32, 32, 32, 48)
+A_ROWS = (32, 32, 48, 32)
 ROWS_OWN = SEQ // NTP
 
 
@@ -55,7 +55,7 @@
     return i.stop - i.start if isinstance(i, slice) else 1
 
 
-def link_plan(near, ahead, hop=2.6, rate=46.6e3, turn=7.5, times=None):
+def link_plan(near, ahead, hop=2.6, rate=46.6e3, times=None):
     table = {(g, *m): v for g in range(4) for m, v in messages(g).items()}
     need = {m: {(m[0], *x) for x in v[4]} for m, v in table.items()}
     feeds, then = {}, {}
@@ -120,8 +120,7 @@
             fill(now + span)
             now += span
             ops.append(("work", name))
-            if gives:
-                coming.append((now + turn, len(ops), gives))
+            coming.extend((now + TURN[x[0]], len(ops), x) for x in gives)
         elif not fill(min(coming)[0] if coming else now + 1e3):
             now = max(now, min(coming)[0])
     if times is not None:
@@ -130,20 +129,32 @@
 
 
 WORK = (
-    ("norm", 0.92, (), None),
-    ("mats", 0.42, (), None),
-    ("project", 1.1, (0,), None),
-    ("prepare", 0.27, (), None),
-    *((f"level{l}", 0.34, (), None) for l in range(LEVELS)),
-    ("attend", 0.5, (), None),
-    ("mix_out", 0.9, (1,), "scatter1"),
-    ("residual", 0.3, ("scatter1",), "spread1"),
-    ("gate_up", 1.1, ("spread1", 2), None),
-    ("hidden", 0.2, (), None),
-    ("down", 1.1, (3,), "scatter2"),
-    ("layer_out", 0.3, ("scatter2",), "spread2"),
-    ("end", 0.1, ("spread2",), None),
+    ("norm", 0.92, (), ()),
+    ("mats", 0.67, (), ()),
+    ("project", 1.1, (0,), ()),
+    ("prepare", 0.27, (), ()),
+    *((f"level{l}", 0.34, (), ()) for l in range(LEVELS)),
+    ("attend", 0.35, (), ()),
+    ("mix0", 0.5, (1,), ("d00",)),
+    ("mix1", 0.5, (), ("d01",)),
+    ("pair00", 0.1, ("d00",), ("x00",)),
+    ("pair01", 0.1, ("d01",), ("x01",)),
+    ("residual", 0.25, ("x00", "x01"), ("s00", "s01")),
+    ("relay00", 0.05, ("s00",), ("f00",)),
+    ("relay01", 0.05, ("s01",), ("f01",)),
+    ("gate_up", 1.1, ("f00", "f01", 2), ()),
+    ("hidden", 0.07, (), ()),
+    ("down0", 0.53, (3,), ("d10",)),
+    ("down1", 0.53, (), ("d11",)),
+    ("pair10", 0.1, ("d10",), ("x10",)),
+    ("pair11", 0.1, ("d11",), ("x11",)),
+    ("layer0", 0.1, ("x10",), ("s10",)),
+    ("layer1", 0.1, ("x11",), ("s11",)),
+    ("relay10", 0.05, ("s10",), ("f10",)),
+    ("relay11", 0.05, ("s11",), ("f11",)),
+    ("end", 0.1, ("f10", "f11"), ()),
 )
+TURN = dict(d=1.4, x=4.6, s=4.6, f=1.4)
 NEAR, AHEAD = 0.5, 12
 
 
@@ -163,10 +174,12 @@
     tok_hbm, gain1, bias, spike, hgain, gain2, wq, wk, wv, wd, wo, wg, wu, wdn,
     out,
     tok, extra, fin,
-    g1, g2, g3, g4, xn, acc, mats, score, att, part, got, n2, acc2, hid, part2, got2, resid, decay2, qf, kf, vbd,
+    g1, g2, g3, g4, xn, acc, mats, score, att, n2, acc2, hid, resid, decay2, qf, kf, vbd,
+    part, part2, land, land2, both1, both2, got, got2,
     lsem, send, recv, tsend, trecv,
 ):
     bufs = (g1, g2, g3, g4)
+    parts, lands, both, gots = (part, part2), (land, land2), (both1, both2), (got, got2)
     rep, f, t = lax.axis_index("rep"), lax.axis_index("fs"), lax.axis_index("tp")
     y, z = lax.rem(f, NY), lax.div(f, NY)
     zz = rep * NZ + z
@@ -180,11 +193,17 @@
 
     ynb, znb = (at_y(1), at_y(-1)), (at_z(1), at_z(-1))
 
+    x, core = lax.div(t, 2), lax.rem(t, 2)
+    partner = (rep, f, t + 1 - 2 * core)
+
+    def around(k):
+        return lax.rem(x + k, NTP // 2)
+
     def peer(k):
-        return (rep, f, lax.rem(t + k, NTP))
+        return (rep, f, 2 * around(k) + core)
 
     barrier = pltpu.get_barrier_semaphore()
-    others = [*ynb, *znb, *(peer(k) for k in range(1, NTP))]
+    others = [*ynb, *znb, partner, *(peer(k) for k in (1, 2, 3))]
     for d in others:
         pl.semaphore_signal(barrier, inc=1, device_id=d, device_id_type=MESH)
 
@@ -303,58 +322,93 @@
         gains = jnp.concatenate([hgain[...]] * HEADS, axis=1)
         att[...] = (mixed * lax.rsqrt(mean + EPS) * gains).astype(BF16)
 
-    def project_out(left, weight, width, into):
+    def cols_of(c):
+        return slice(c * D // 2, (c + 1) * D // 2)
+
+    def copy_to(device, n, src, dst, sem):
+        pltpu.make_async_remote_copy(
+            src_ref=src, dst_ref=dst, send_sem=tsend.at[n], recv_sem=sem, device_id=device, device_id_type=MESH
+        ).start()
+
+    def project_out(n, c, left, weight, width):
+        into = parts[n]
+
+        def body(w, carry):
+            cols = pl.ds(pl.multiple_of(w * 512, 512), 512)
+            value = dot_t(left[...], weight[w].reshape(512, width)).astype(BF16)
+            into[:, :, :, cols] = value.reshape(NTP // 2, 2, ROWS_OWN, 512)
+            return carry
+
+        lax.fori_loop(2 * c, 2 * c + 2, body, 0)
+        cols = cols_of(c)
+        copy_to(partner, n, into.at[:, 1 - core, :, cols], lands[n].at[:, :, cols], trecv.at[n, 0, c])
+
+    def pair(n, c):
+        cols = cols_of(c)
+        both[n][:, :, cols] = (
+            parts[n][:, core, :, cols].astype(F32) + lands[n][:, :, cols].astype(F32)
+        ).astype(BF16)
+        for k in (1, 2, 3):
+            copy_to(peer(k), n, both[n].at[around(k), :, cols], gots[n].at[k - 1, :, cols], trecv.at[n, 1, c])
+
+    def total(n, cols):
+        s = parts[n][x, core, :, cols].astype(F32) + lands[n][x, :, cols].astype(F32)
+        for k in range(3):
+            s = s + gots[n][k, :, cols].astype(F32)
+        return s
+
+    own_rows = pl.ds(pl.multiple_of(t * ROWS_OWN, ROWS_OWN), ROWS_OWN)
+
+    def residual_rows():
+        r = (tok[own_rows, :].astype(F32) + total(0, slice(0, D))).astype(BF16).astype(F32)
+        resid[...] = r
+        n2[x, core] = (r * lax.rsqrt(jnp.mean(r * r, axis=-1, keepdims=True) + EPS) * gain2[...]).astype(BF16)
+        for c in (0, 1):
+            mine = n2.at[x, core, :, cols_of(c)]
+            for k in (1, 2, 3):
+                copy_to(peer(k), 0, mine, mine, trecv.at[0, 2, c])
+            copy_to(partner, 0, mine, mine, trecv.at[0, 3, c])
+
+    def relay_normed(c):
+        for k in (1, 2, 3):
+            piece = n2.at[around(k), core, :, cols_of(c)]
+            copy_to(partner, 0, piece, piece, trecv.at[0, 3, c])
+
+    def out_at(i, c):
+        rows = pl.ds(pl.multiple_of((2 * i + core) * ROWS_OWN, ROWS_OWN), ROWS_OWN)
+        return out.at[rows, cols_of(c)]
+
+    def put(i, c):
+        piece = fin.at[i, :, cols_of(c)]
+        copy_to(partner, 1, piece, out_at(i, c), trecv.at[1, 3, c])
+        pltpu.make_async_copy(piece, out_at(i, c), lsem.at[5]).start()
+
+    def layer_out(c):
+        cols = cols_of(c)
+        fin[x, :, cols] = (resid[:, cols] + total(1, cols)).astype(BF16)
+        for k in (1, 2, 3):
+            copy_to(peer(k), 1, fin.at[x, :, cols], fin.at[x, :, cols], trecv.at[1, 2, c])
+        put(x, c)
+
+    def relay_out(c):
+        for k in (1, 2, 3):
+            put(around(k), c)
+
+    def end():
+        wait_bytes(fin, lsem.at[5])
+
+    def take_exchange(what):
+        n, c = int(what[1]), int(what[2])
+        kind = "dxsf".index(what[0])
+        ref = lands[n].at[:, :, cols_of(c)] if what[0] in "df" else gots[n].at[:, :, cols_of(c)]
+        wait_bytes(ref, trecv.at[n, kind, c])
+
+    def gate_up():
+        acc2[...] = jnp.zeros_like(acc2)
+
         def body(w, c):
             cols = pl.ds(pl.multiple_of(w * 512, 512), 512)
-            into[:, cols] = dot_t(left[...], weight[w].reshape(512, width)).astype(BF16)
-            return c
-
-        lax.fori_loop(0, NZ, body, 0)
-
-    def rows_of(k):
-        return pl.ds(pl.multiple_of(lax.rem(t + k + NTP, NTP) * ROWS_OWN, ROWS_OWN), ROWS_OWN)
-
-    own_rows = rows_of(0)
-
-    def exchange(n, k, src, dst):
-        pltpu.make_async_remote_copy(
-            src_ref=src, dst_ref=dst, send_sem=tsend.at[n], recv_sem=trecv.at[n],
-            device_id=peer(k), device_id_type=MESH,
-        ).start()
-
-    def scatter(n, src, dst):
-        for k in range(1, NTP):
-            exchange(n, k, src.at[rows_of(k), :], dst.at[k])
-
-    def spread(n, src, ref):
-        for k in range(1, NTP):
-            exchange(n, k, src, ref.at[own_rows, :])
-
-    def exchange_wait(n, sem):
-        wait_bytes(part.at[0 : SEQ - ROWS_OWN, :], sem.at[n])
-
-    def total(src, dst):
-        s = src[own_rows, :].astype(F32)
-        for k in range(1, NTP):
-            s = s + dst[k].astype(F32)
-        return s
-
-    def mix_out():
-        project_out(att, g2, 256, part)
-        scatter(0, part, got)
-
-    def residual_rows():
-        r = (tok[own_rows, :].astype(F32) + total(part, got)).astype(BF16).astype(F32)
-        resid[...] = r
-        n2[own_rows, :] = (r * lax.rsqrt(jnp.mean(r * r, axis=-1, keepdims=True) + EPS) * gain2[...]).astype(BF16)
-        spread(1, n2.at[own_rows, :], n2)
-
-    def gate_up():
-        acc2[...] = jnp.zeros_like(acc2)
-
-        def body(w, c):
-            cols = pl.ds(pl.multiple_of(w * 512, 512), 512)
-            acc2[...] += dot(n2[:, cols], g3[w].reshape(512, 768))
+            acc2[...] += dot(n2[:, :, :, cols].reshape(SEQ, 512), g3[w].reshape(512, 768))
             return c
 
         lax.fori_loop(0, NZ, body, 0)
@@ -363,26 +417,18 @@
         gated = acc2[:, 0:384]
         hid[...] = (gated / (1.0 + jnp.exp(-gated)) * acc2[:, 384:768]).astype(BF16)
 
-    def down():
-        project_out(hid, g4, 384, part2)
-        scatter(2, part2, got2)
-
-    own_out = pltpu.make_async_copy(fin, out.at[own_rows, :], lsem.at[5])
-
-    def layer_out():
-        fin[...] = (resid[...] + total(part2, got2)).astype(BF16)
-        spread(3, fin, out)
-        own_out.start()
-
-    def end():
-        own_out.wait()
-
     work = dict(
-        norm=norm, mats=build, project=project, prepare=prepare, attend=attend, mix_out=mix_out,
-        residual=residual_rows, gate_up=gate_up, hidden=hidden, down=down, layer_out=layer_out, end=end,
+        norm=norm, mats=build, project=project, prepare=prepare, attend=attend,
+        residual=residual_rows, gate_up=gate_up, hidden=hidden, end=end,
         **{f"level{l}": functools.partial(level, l) for l in range(LEVELS)},
+        **{f"pair{n}{c}": functools.partial(pair, n, c) for n in (0, 1) for c in (0, 1)},
     )
-    turns = dict(scatter1=0, spread1=1, scatter2=2, spread2=3)
+    for c in (0, 1):
+        work[f"mix{c}"] = functools.partial(project_out, 0, c, att, g2, 256)
+        work[f"down{c}"] = functools.partial(project_out, 1, c, hid, g4, 384)
+        work[f"relay0{c}"] = functools.partial(relay_normed, c)
+        work[f"relay1{c}"] = functools.partial(relay_out, c)
+        work[f"layer{c}"] = functools.partial(layer_out, c)
     waiting = set(range(4))
     for verb, what in link_plan(NEAR, AHEAD):
         with jax.named_scope(f"{verb}_{what}".replace(" ", "")):
@@ -394,13 +440,15 @@
                     own[what[0]].wait()
                 send_weight(*what)
             elif isinstance(what, str):
-                exchange_wait(turns[what], trecv)
+                take_exchange(what)
             else:
                 take_weight(*what)
     for g in range(4):
         wait_bytes(bufs[g].at[0:3], send.at[g])
         wait_bytes(bufs[g].at[3, 0:7], send.at[g])
-        exchange_wait(g, tsend)
+    for n in (0, 1):
+        wait_bytes(parts[n], tsend.at[n])
+        wait_bytes(parts[n].at[0:3], tsend.at[n])
 
 
 def shards(
@@ -418,30 +466,29 @@
         scratch_shapes=[
             pltpu.VMEM((SEQ, D), BF16),
             pltpu.VMEM((SEQ, 128), F32),
-            pltpu.VMEM((ROWS_OWN, D), BF16),
+            pltpu.VMEM((NTP // 2, ROWS_OWN, D), BF16),
             *(pltpu.VMEM((NZ, NY, SLAB, w), BF16) for w in widths),
             pltpu.VMEM((SEQ, D), BF16),
             pltpu.VMEM((SEQ, 640), F32),
             pltpu.VMEM((2 * LEVELS, SEQ, 2 * SEQ), BF16),
             pltpu.VMEM((SEQ, HEADS * SEQ), F32),
             pltpu.VMEM((SEQ, 256), BF16),
-            pltpu.VMEM((SEQ, D), BF16),
-            pltpu.VMEM((NTP, ROWS_OWN, D), BF16),
-            pltpu.VMEM((SEQ, D), BF16),
+            pltpu.VMEM((NTP // 2, 2, ROWS_OWN, D), BF16),
             pltpu.VMEM((SEQ, 768), F32),
             pltpu.VMEM((SEQ, 384), BF16),
-            pltpu.VMEM((SEQ, D), BF16),
-            pltpu.VMEM((NTP, ROWS_OWN, D), BF16),
             pltpu.VMEM((ROWS_OWN, D), F32),
             pltpu.VMEM((2 * SEQ, 128), BF16),
             pltpu.VMEM((SEQ, 128), F32),
             pltpu.VMEM((SEQ, 128), F32),
             pltpu.VMEM((HEADS * SEQ, 256), BF16),
+            *[pltpu.VMEM((NTP // 2, 2, ROWS_OWN, D), BF16)] * 2,
+            *[pltpu.VMEM((NTP // 2, ROWS_OWN, D), BF16)] * 4,
+            *[pltpu.VMEM((NTP // 2 - 1, ROWS_OWN, D), BF16)] * 2,
             pltpu.SemaphoreType.DMA((6,)),
             pltpu.SemaphoreType.DMA((4,)),
             pltpu.SemaphoreType.DMA((4, len(TAKES))),
-            pltpu.SemaphoreType.DMA((4,)),
-            pltpu.SemaphoreType.DMA((4,)),
+            pltpu.SemaphoreType.DMA((2,)),
+            pltpu.SemaphoreType.DMA((2, 4, 2)),
         ],
         compiler_params=pltpu.CompilerParams(collective_id=0, has_side_effects=True),
     )(

time: 86.5 us -> 80.1 us (0.926)
  Pallas kernels: 84.4 us -> 78 us
    pallas_call x1, Pallas kernels: 84.4 us -> 78 us  [shards(): pl.pallas_call(layer_kernel, out_shape=jax.ShapeDtypeStruct((SEQ, D), BF1...]
where the time goes in v4:
time: 80.1 us; the launch traced here: 79.9 us
  Pallas kernels  78 us (97%)
  local copies, waits for them, and re-layouts  1.88 us (2%)
    pallas_call x1, Pallas kernels, shards(): pl.pallas_call(layer_kernel, out_shape=jax.ShapeDtypeStruct((SEQ, D), BF1...  78 us
    unnamed x1, local copies, waits for them, and re-layouts  1.88 us

profile of v4, /device:TPU:1, one launch (start us, length us, event | category | flops | bytes accessed | tf_op | source)
XLA Modules:
  0.0 79.9 jit_solution(16951092006696747425)
XLA Ops:
  0.0 78.0 %shard_map.136 = bf16[128,2048]{1,0:T(8,128)(2,1)} custom-call(bf16[128,2048]{1,0:T(8,128)(2,1)} %tok_hbm.1, f32[1,2048]{1,0:T(1,128)} %bitcast.5, f32[1,128]{1,0:T(1,128)} %bitcast.8, f32[4,128]{1,0:T(4,128)} %bitcast.7, f32[1,64]{1,0:T(1,128)} %bitcast.9, f32[1,2048]{1,0:T(1,128)} %bitcast.6, bf16[64,128]{1,0:T(8,128)(2,1)} %wq.1, bf16[64,128]{1,0:T(8,128)(2,1)} %wk.1, ...), custom_call_target="tpu_custom_call" | custom-call | tf_op jit(solution)/shard_map/pallas_call | solution.py:461
  78.0 1.9 %copy.16 = bf16[128,2048]{1,0:T(8,128)(2,1)} copy(bf16[128,2048]{1,0:T(8,128)(2,1)} %shard_map.136) | data formatting | bytes 1048576

commit v5 on v4

--- a/solution.py
+++ b/solution.py
@@ -16,8 +16,10 @@
 LEVELS = 7
 EPS = 1e-6
 PARTS = ((128, 128, 256, 128), (256,), (384, 384), (384,))
-A_ROWS = (32, 32, 48, 32)
+A_ROWS = (32, 48, 32, 64)
 ROWS_OWN = SEQ // NTP
+CHUNKS = NZ
+SLAB_ORDER = (0, -1, 1, 2)
 
 
 def messages(g):
@@ -45,7 +47,7 @@
                     "y", half, back * s, rows_b, (("by", 2 * s - 3 + h if s > 1 else 0),), ("by", 2 * s - 1 + h),
                 )
         out["by", d, 8] = ("y", slice(2 * d, 2 * d + 2), back * 3, rows_b, (("by", 3 + d),), ("by", 5))
-    return out
+    return {m: v for m, v in out.items() if extent(v[3])}
 
 
 TAKES = [("ay", 0), ("ay", 1), ("ay", 2), ("ay", 3), ("az", 0), ("az", 1), ("bz", 0), ("bz", 1), *(("by", i) for i in range(6))]
@@ -55,7 +57,7 @@
     return i.stop - i.start if isinstance(i, slice) else 1
 
 
-def link_plan(near, ahead, hop=2.6, rate=46.6e3, times=None):
+def link_plan(near, hop=2.4, rate=46.6e3, times=None):
     table = {(g, *m): v for g in range(4) for m, v in messages(g).items()}
     need = {m: {(m[0], *x) for x in v[4]} for m, v in table.items()}
     feeds, then = {}, {}
@@ -67,7 +69,7 @@
     def urgency(m):
         g, name, d, i = m
         second = name == "by" or name == "az"
-        return (g * 10 - (0 if second else ahead), i, d)
+        return (BASE[g] if second else LIGHT[g], i, d)
 
     ready = {(a, d): [] for a in ("y", "z") for d in (0, 1)}
     free = dict.fromkeys(ready, 0.0)
@@ -75,7 +77,7 @@
     for m, v in table.items():
         if not need[m]:
             ready[v[0], m[2]].append(m)
-    now, ops, have, coming, at = 0.2, [], set(), [], 0
+    now, ops, have, coming, todo = 0.2, [], set(), [], list(WORK)
     landed = {}
     def fill(until):
         nonlocal now
@@ -95,15 +97,15 @@
                 now += 0.02
         return len(ops) > before
 
-    while at < len(WORK) or coming:
+    while todo or coming:
         fill(now + near)
         coming.sort()
         if coming and coming[0][0] <= now:
             m = coming.pop(0)[2]
             ops.append(("take", m))
             now += 0.02
+            have.add(m)
             if isinstance(m, str):
-                have.add(m)
                 continue
             left[m[0]] -= 1
             if left[m[0]] == 0:
@@ -114,9 +116,12 @@
                 need[x].discard(m)
                 if not need[x]:
                     ready[table[x][0], x[2]].append(x)
-        elif at < len(WORK) and all(q in have for q in WORK[at][2]):
-            name, span, _, gives = WORK[at]
-            at += 1
+            continue
+        item = next((w for w in todo if all(q in have for q in w[2])), None)
+        if item:
+            todo.remove(item)
+            name, span, _, gives = item
+            have.add(name)
             fill(now + span)
             now += span
             ops.append(("work", name))
@@ -128,34 +133,30 @@
     return ops
 
 
+EACH = range(CHUNKS)
+LAST = ((3, "ay", 0), (3, "ay", 1), (3, "ay", 2), (3, "ay", 3)), ((3, "az", 0),), ((3, "az", 0),), ((3, "az", 1),)
 WORK = (
     ("norm", 0.92, (), ()),
     ("mats", 0.67, (), ()),
-    ("project", 1.1, (0,), ()),
-    ("prepare", 0.27, (), ()),
-    *((f"level{l}", 0.34, (), ()) for l in range(LEVELS)),
-    ("attend", 0.35, (), ()),
-    ("mix0", 0.5, (1,), ("d00",)),
-    ("mix1", 0.5, (), ("d01",)),
-    ("pair00", 0.1, ("d00",), ("x00",)),
-    ("pair01", 0.1, ("d01",), ("x01",)),
-    ("residual", 0.25, ("x00", "x01"), ("s00", "s01")),
-    ("relay00", 0.05, ("s00",), ("f00",)),
-    ("relay01", 0.05, ("s01",), ("f01",)),
-    ("gate_up", 1.1, ("f00", "f01", 2), ()),
-    ("hidden", 0.07, (), ()),
-    ("down0", 0.53, (3,), ("d10",)),
-    ("down1", 0.53, (), ("d11",)),
-    ("pair10", 0.1, ("d10",), ("x10",)),
-    ("pair11", 0.1, ("d11",), ("x11",)),
-    ("layer0", 0.1, ("x10",), ("s10",)),
-    ("layer1", 0.1, ("x11",), ("s11",)),
-    ("relay10", 0.05, ("s10",), ("f10",)),
-    ("relay11", 0.05, ("s11",), ("f11",)),
-    ("end", 0.1, ("f10", "f11"), ()),
+    ("project", 1.1, ("norm", 0), ()),
+    ("prepare", 0.27, ("project", "mats"), ()),
+    *((f"level{l}", 0.34, (f"level{l - 1}" if l else "prepare",), ()) for l in range(LEVELS)),
+    ("attend", 0.36, (f"level{LEVELS - 1}",), ()),
+    *((f"mix{c}", 0.23, ("attend", 1), (f"d0{c}",)) for c in EACH),
+    *((f"pair0{c}", 0.05, (f"d0{c}",), (f"x0{c}",)) for c in EACH),
+    ("residual", 0.2, tuple(f"x0{c}" for c in EACH), tuple(f"s0{c}" for c in EACH)),
+    *((f"relay0{c}", 0.03, (f"s0{c}",), (f"f0{c}",)) for c in EACH),
+    ("gate_up", 1.12, (*(f"f0{c}" for c in EACH), *(f"relay0{c}" for c in EACH), 2), ()),
+    ("hidden", 0.07, ("gate_up",), ()),
+    *((f"down{c}", 0.27, ("hidden", *LAST[c]), (f"d1{c}",)) for c in EACH),
+    *((f"pair1{c}", 0.05, (f"d1{c}",), (f"x1{c}",)) for c in EACH),
+    *((f"layer{c}", 0.05, (f"x1{c}",), (f"s1{c}",)) for c in EACH),
+    *((f"relay1{c}", 0.03, (f"s1{c}",), (f"f1{c}",)) for c in EACH),
+    ("end", 0.1, (*(f"f1{c}" for c in EACH), *(f"relay1{c}" for c in EACH)), ()),
 )
-TURN = dict(d=1.4, x=4.6, s=4.6, f=1.4)
-NEAR, AHEAD = 0.5, 12
+TURN = dict(d=1.3, x=4.9, s=4.4, f=1.3)
+NEAR = 0.3
+BASE, LIGHT = (0, -1, 20, 22), (-12, -13, 2, 19)
 
 
 def dot(a, b):
@@ -171,9 +172,9 @@
 
 
 def layer_kernel(
-    tok_hbm, gain1, bias, spike, hgain, gain2, wq, wk, wv, wd, wo, wg, wu, wdn,
+    tok_hbm, gain1_hbm, bias_hbm, spike_hbm, hgain_hbm, gain2_hbm, wq, wk, wv, wd, wo, wg, wu, wdn,
     out,
-    tok, extra, fin,
+    tok, gain1, bias, spike, hgain, gain2, extra, fin,
     g1, g2, g3, g4, xn, acc, mats, score, att, n2, acc2, hid, resid, decay2, qf, kf, vbd,
     part, part2, land, land2, both1, both2, got, got2,
     lsem, send, recv, tsend, trecv,
@@ -218,8 +219,12 @@
             c.start()
         own.append(pltpu.make_async_copy(bufs[g].at[z, y], bufs[g].at[z, y], lsem.at[g]))
         if g == 0:
-            tok_copy = pltpu.make_async_copy(tok_hbm, tok, lsem.at[4])
-            tok_copy.start()
+            small = ((gain1_hbm, gain1), (bias_hbm, bias), (spike_hbm, spike), (hgain_hbm, hgain), (gain2_hbm, gain2))
+            fetches = [
+                pltpu.make_async_copy(src, dst, lsem.at[6 + i]) for i, (src, dst) in enumerate(((tok_hbm, tok), *small))
+            ]
+            for c in fetches:
+                c.start()
 
     pl.semaphore_wait(barrier, len(others))
 
@@ -259,7 +264,8 @@
         return c
 
     def norm():
-        tok_copy.wait()
+        for c in fetches:
+            c.wait()
         lax.fori_loop(0, SEQ // 16, norm_rows, 0)
 
     def build_mats(l, c):
@@ -323,24 +329,20 @@
         att[...] = (mixed * lax.rsqrt(mean + EPS) * gains).astype(BF16)
 
     def cols_of(c):
-        return slice(c * D // 2, (c + 1) * D // 2)
+        return slice(c * D // CHUNKS, (c + 1) * D // CHUNKS)
 
     def copy_to(device, n, src, dst, sem):
         pltpu.make_async_remote_copy(
             src_ref=src, dst_ref=dst, send_sem=tsend.at[n], recv_sem=sem, device_id=device, device_id_type=MESH
         ).start()
 
+    def slab_of(c):
+        return lax.rem(z + SLAB_ORDER[c] + NZ, NZ)
+
     def project_out(n, c, left, weight, width):
-        into = parts[n]
-
-        def body(w, carry):
-            cols = pl.ds(pl.multiple_of(w * 512, 512), 512)
-            value = dot_t(left[...], weight[w].reshape(512, width)).astype(BF16)
-            into[:, :, :, cols] = value.reshape(NTP // 2, 2, ROWS_OWN, 512)
-            return carry
-
-        lax.fori_loop(2 * c, 2 * c + 2, body, 0)
-        cols = cols_of(c)
+        into, cols = parts[n], cols_of(c)
+        rows = weight[c if n == 0 else slab_of(c)].reshape(D // NZ, width)
+        into[:, :, :, cols] = dot_t(left[...], rows).astype(BF16).reshape(NTP // 2, 2, ROWS_OWN, D // NZ)
         copy_to(partner, n, into.at[:, 1 - core, :, cols], lands[n].at[:, :, cols], trecv.at[n, 0, c])
 
     def pair(n, c):
@@ -363,7 +365,7 @@
         r = (tok[own_rows, :].astype(F32) + total(0, slice(0, D))).astype(BF16).astype(F32)
         resid[...] = r
         n2[x, core] = (r * lax.rsqrt(jnp.mean(r * r, axis=-1, keepdims=True) + EPS) * gain2[...]).astype(BF16)
-        for c in (0, 1):
+        for c in range(CHUNKS):
             mine = n2.at[x, core, :, cols_of(c)]
             for k in (1, 2, 3):
                 copy_to(peer(k), 0, mine, mine, trecv.at[0, 2, c])
@@ -374,9 +376,12 @@
             piece = n2.at[around(k), core, :, cols_of(c)]
             copy_to(partner, 0, piece, piece, trecv.at[0, 3, c])
 
+    def place_of(c):
+        return pl.ds(pl.multiple_of(slab_of(c) * (D // NZ), D // NZ), D // NZ)
+
     def out_at(i, c):
         rows = pl.ds(pl.multiple_of((2 * i + core) * ROWS_OWN, ROWS_OWN), ROWS_OWN)
-        return out.at[rows, cols_of(c)]
+        return out.at[rows, place_of(c)]
 
     def put(i, c):
         piece = fin.at[i, :, cols_of(c)]
@@ -384,8 +389,8 @@
         pltpu.make_async_copy(piece, out_at(i, c), lsem.at[5]).start()
 
     def layer_out(c):
-        cols = cols_of(c)
-        fin[x, :, cols] = (resid[:, cols] + total(1, cols)).astype(BF16)
+        cols, at = cols_of(c), place_of(c)
+        fin[x, :, cols] = (resid[:, at] + total(1, cols)).astype(BF16)
         for k in (1, 2, 3):
             copy_to(peer(k), 1, fin.at[x, :, cols], fin.at[x, :, cols], trecv.at[1, 2, c])
         put(x, c)
@@ -421,16 +426,16 @@
         norm=norm, mats=build, project=project, prepare=prepare, attend=attend,
         residual=residual_rows, gate_up=gate_up, hidden=hidden, end=end,
         **{f"level{l}": functools.partial(level, l) for l in range(LEVELS)},
-        **{f"pair{n}{c}": functools.partial(pair, n, c) for n in (0, 1) for c in (0, 1)},
+        **{f"pair{n}{c}": functools.partial(pair, n, c) for n in (0, 1) for c in range(CHUNKS)},
     )
-    for c in (0, 1):
+    for c in range(CHUNKS):
         work[f"mix{c}"] = functools.partial(project_out, 0, c, att, g2, 256)
         work[f"down{c}"] = functools.partial(project_out, 1, c, hid, g4, 384)
         work[f"relay0{c}"] = functools.partial(relay_normed, c)
         work[f"relay1{c}"] = functools.partial(relay_out, c)
         work[f"layer{c}"] = functools.partial(layer_out, c)
     waiting = set(range(4))
-    for verb, what in link_plan(NEAR, AHEAD):
+    for verb, what in link_plan(NEAR):
         with jax.named_scope(f"{verb}_{what}".replace(" ", "")):
             if verb == "work":
                 work[what]()
@@ -455,16 +460,20 @@
     tokens, attention_norm_gain, query_weight, key_weight, value_weight, decay_weight, decay_gate_bias,
     decay_spike_extra, head_output_gain, output_weight, channel_norm_gain, gate_weight, up_weight, down_weight,
 ):
-    vmem = pl.BlockSpec(memory_space=pltpu.VMEM)
-    hbm = pl.BlockSpec(memory_space=pl.ANY)
+    hbm = pl.BlockSpec(memory_space=pltpu.HBM)
     widths = [sum(p) for p in PARTS]
     return pl.pallas_call(
         layer_kernel,
         out_shape=jax.ShapeDtypeStruct((SEQ, D), BF16),
-        in_specs=[hbm] + [vmem] * 5 + [hbm] * 8,
-        out_specs=hbm,
+        in_specs=[hbm] * 14,
+        out_specs=pl.BlockSpec(memory_space=pl.ANY),
         scratch_shapes=[
             pltpu.VMEM((SEQ, D), BF16),
+            pltpu.VMEM((1, D), F32),
+            pltpu.VMEM((1, 128), F32),
+            pltpu.VMEM((HEADS, SEQ), F32),
+            pltpu.VMEM((1, VW), F32),
+            pltpu.VMEM((1, D), F32),
             pltpu.VMEM((SEQ, 128), F32),
             pltpu.VMEM((NTP // 2, ROWS_OWN, D), BF16),
             *(pltpu.VMEM((NZ, NY, SLAB, w), BF16) for w in widths),
@@ -484,11 +493,11 @@
             *[pltpu.VMEM((NTP // 2, 2, ROWS_OWN, D), BF16)] * 2,
             *[pltpu.VMEM((NTP // 2, ROWS_OWN, D), BF16)] * 4,
             *[pltpu.VMEM((NTP // 2 - 1, ROWS_OWN, D), BF16)] * 2,
-            pltpu.SemaphoreType.DMA((6,)),
+            pltpu.SemaphoreType.DMA((12,)),
             pltpu.SemaphoreType.DMA((4,)),
             pltpu.SemaphoreType.DMA((4, len(TAKES))),
             pltpu.SemaphoreType.DMA((2,)),
-            pltpu.SemaphoreType.DMA((2, 4, 2)),
+            pltpu.SemaphoreType.DMA((2, 4, CHUNKS)),
         ],
         compiler_params=pltpu.CompilerParams(collective_id=0, has_side_effects=True),
     )(

time: 80.1 us -> 77.9 us (0.973)
  Pallas kernels: 78 us -> 75.8 us
    pallas_call x1, Pallas kernels: 78 us -> 75.8 us  [shards(): pl.pallas_call(layer_kernel, out_shape=jax.ShapeDtypeStruct((SEQ, D), BF1...]
where the time goes in v5:
time: 77.9 us; the launch traced here: 77.7 us
  Pallas kernels  75.8 us (97%)
  local copies, waits for them, and re-layouts  1.88 us (2%)
    pallas_call x1, Pallas kernels, shards(): pl.pallas_call(layer_kernel, out_shape=jax.ShapeDtypeStruct((SEQ, D), BF1...  75.8 us
    unnamed x1, local copies, waits for them, and re-layouts  1.88 us

profile of v5, /device:TPU:1, one launch (start us, length us, event | category | flops | bytes accessed | tf_op | source)
XLA Modules:
  0.0 77.7 jit_solution(13843995617459556319)
XLA Ops:
  0.0 75.8 %shard_map.136 = bf16[128,2048]{1,0:T(8,128)(2,1)} custom-call(bf16[128,2048]{1,0:T(8,128)(2,1)} %tok_hbm.1, f32[1,2048]{1,0:T(1,128)} %bitcast.5, f32[1,128]{1,0:T(1,128)} %bitcast.8, f32[4,128]{1,0:T(4,128)} %bitcast.7, f32[1,64]{1,0:T(1,128)} %bitcast.9, f32[1,2048]{1,0:T(1,128)} %bitcast.6, bf16[64,128]{1,0:T(8,128)(2,1)} %wq.1, bf16[64,128]{1,0:T(8,128)(2,1)} %wk.1, ...), custom_call_target="tpu_custom_call" | custom-call | tf_op jit(solution)/shard_map/pallas_call | solution.py:465
  75.8 1.9 %copy.16 = bf16[128,2048]{1,0:T(8,128)(2,1)} copy(bf16[128,2048]{1,0:T(8,128)(2,1)} %shard_map.136) | data formatting | bytes 1048576

commit v6 on v5

--- a/solution.py
+++ b/solution.py
@@ -140,11 +140,12 @@
     ("mats", 0.67, (), ()),
     ("project", 1.1, ("norm", 0), ()),
     ("prepare", 0.27, ("project", "mats"), ()),
-    *((f"level{l}", 0.34, (f"level{l - 1}" if l else "prepare",), ()) for l in range(LEVELS)),
-    ("attend", 0.36, (f"level{LEVELS - 1}",), ()),
+    ("levels0", 1.2, ("prepare",), ()),
+    ("levels1", 0.9, ("levels0",), ()),
+    ("attend", 0.36, ("levels1",), ()),
     *((f"mix{c}", 0.23, ("attend", 1), (f"d0{c}",)) for c in EACH),
     *((f"pair0{c}", 0.05, (f"d0{c}",), (f"x0{c}",)) for c in EACH),
-    ("residual", 0.2, tuple(f"x0{c}" for c in EACH), tuple(f"s0{c}" for c in EACH)),
+    *((f"residual{c}", 0.08, (f"x0{c}", *((f"residual{c - 1}",) if c else ())), (f"s0{c}",)) for c in EACH),
     *((f"relay0{c}", 0.03, (f"s0{c}",), (f"f0{c}",)) for c in EACH),
     ("gate_up", 1.12, (*(f"f0{c}" for c in EACH), *(f"relay0{c}" for c in EACH), 2), ()),
     ("hidden", 0.07, ("gate_up",), ()),
@@ -176,7 +177,7 @@
     out,
     tok, gain1, bias, spike, hgain, gain2, extra, fin,
     g1, g2, g3, g4, xn, acc, mats, score, att, n2, acc2, hid, resid, decay2, qf, kf, vbd,
-    part, part2, land, land2, both1, both2, got, got2,
+    part, part2, land, land2, both1, both2, got, got2, factors,
     lsem, send, recv, tsend, trecv,
 ):
     bufs = (g1, g2, g3, g4)
@@ -361,20 +362,30 @@
 
     own_rows = pl.ds(pl.multiple_of(t * ROWS_OWN, ROWS_OWN), ROWS_OWN)
 
-    def residual_rows():
-        r = (tok[own_rows, :].astype(F32) + total(0, slice(0, D))).astype(BF16).astype(F32)
-        resid[...] = r
-        n2[x, core] = (r * lax.rsqrt(jnp.mean(r * r, axis=-1, keepdims=True) + EPS) * gain2[...]).astype(BF16)
-        for c in range(CHUNKS):
-            mine = n2.at[x, core, :, cols_of(c)]
+    def residual(c):
+        cols = cols_of(c)
+        r = (tok[own_rows, cols].astype(F32) + total(0, cols)).astype(BF16).astype(F32)
+        resid[:, cols] = r
+        mine = n2.at[x, core, :, cols]
+        mine[...] = (r * gain2[:, cols]).astype(BF16)
+        pieces = [mine]
+        if c == CHUNKS - 1:
+            r = resid[...]
+            factor = lax.rsqrt(jnp.mean(r * r, axis=-1, keepdims=True) + EPS)
+            factors[x, core] = jnp.broadcast_to(factor, (ROWS_OWN, 128))
+            pieces.append(factors.at[x, core])
+        for piece in pieces:
             for k in (1, 2, 3):
-                copy_to(peer(k), 0, mine, mine, trecv.at[0, 2, c])
-            copy_to(partner, 0, mine, mine, trecv.at[0, 3, c])
+                copy_to(peer(k), 0, piece, piece, trecv.at[0, 2, c])
+            copy_to(partner, 0, piece, piece, trecv.at[0, 3, c])
 
     def relay_normed(c):
         for k in (1, 2, 3):
             piece = n2.at[around(k), core, :, cols_of(c)]
             copy_to(partner, 0, piece, piece, trecv.at[0, 3, c])
+            if c == CHUNKS - 1:
+                piece = factors.at[around(k), core]
+                copy_to(partner, 0, piece, piece, trecv.at[0, 3, c])
 
     def place_of(c):
         return pl.ds(pl.multiple_of(slab_of(c) * (D // NZ), D // NZ), D // NZ)
@@ -405,7 +416,8 @@
     def take_exchange(what):
         n, c = int(what[1]), int(what[2])
         kind = "dxsf".index(what[0])
-        ref = lands[n].at[:, :, cols_of(c)] if what[0] in "df" else gots[n].at[:, :, cols_of(c)]
+        wide = D // CHUNKS + (256 if n == 0 and what[0] in "sf" and c == CHUNKS - 1 else 0)
+        ref = (lands if what[0] in "df" else gots)[n].at[:, :, 0:wide]
         wait_bytes(ref, trecv.at[n, kind, c])
 
     def gate_up():
@@ -419,18 +431,20 @@
         lax.fori_loop(0, NZ, body, 0)
 
     def hidden():
-        gated = acc2[:, 0:384]
-        hid[...] = (gated / (1.0 + jnp.exp(-gated)) * acc2[:, 384:768]).astype(BF16)
+        factor = factors[...].reshape(SEQ, 128)[:, 0:1]
+        gated = acc2[:, 0:384] * factor
+        hid[...] = (gated / (1.0 + jnp.exp(-gated)) * (acc2[:, 384:768] * factor)).astype(BF16)
 
     work = dict(
         norm=norm, mats=build, project=project, prepare=prepare, attend=attend,
-        residual=residual_rows, gate_up=gate_up, hidden=hidden, end=end,
-        **{f"level{l}": functools.partial(level, l) for l in range(LEVELS)},
+        gate_up=gate_up, hidden=hidden, end=end,
+        levels0=lambda: [level(l) for l in range(4)], levels1=lambda: [level(l) for l in range(4, LEVELS)],
         **{f"pair{n}{c}": functools.partial(pair, n, c) for n in (0, 1) for c in range(CHUNKS)},
     )
     for c in range(CHUNKS):
         work[f"mix{c}"] = functools.partial(project_out, 0, c, att, g2, 256)
         work[f"down{c}"] = functools.partial(project_out, 1, c, hid, g4, 384)
+        work[f"residual{c}"] = functools.partial(residual, c)
         work[f"relay0{c}"] = functools.partial(relay_normed, c)
         work[f"relay1{c}"] = functools.partial(relay_out, c)
         work[f"layer{c}"] = functools.partial(layer_out, c)
@@ -454,6 +468,8 @@
     for n in (0, 1):
         wait_bytes(parts[n], tsend.at[n])
         wait_bytes(parts[n].at[0:3], tsend.at[n])
+    wait_bytes(factors.at[0:3], tsend.at[0])
+    wait_bytes(factors.at[3, 0], tsend.at[0])
 
 
 def shards(
@@ -493,6 +509,7 @@
             *[pltpu.VMEM((NTP // 2, 2, ROWS_OWN, D), BF16)] * 2,
             *[pltpu.VMEM((NTP // 2, ROWS_OWN, D), BF16)] * 4,
             *[pltpu.VMEM((NTP // 2 - 1, ROWS_OWN, D), BF16)] * 2,
+            pltpu.VMEM((NTP // 2, 2, ROWS_OWN, 128), F32),
             pltpu.SemaphoreType.DMA((12,)),
             pltpu.SemaphoreType.DMA((4,)),
             pltpu.SemaphoreType.DMA((4, len(TAKES))),

time: 77.9 us -> 77.5 us (level)
  no operation moved by 1% of the time
where the time goes in v6:
time: 77.5 us; the launch traced here: 77.3 us
  Pallas kernels  75.4 us (97%)
  local copies, waits for them, and re-layouts  1.88 us (2%)
    pallas_call x1, Pallas kernels, shards(): pl.pallas_call(layer_kernel, out_shape=jax.ShapeDtypeStruct((SEQ, D), BF1...  75.4 us
    unnamed x1, local copies, waits for them, and re-layouts  1.88 us

profile of v6, /device:TPU:1, one launch (start us, length us, event | category | flops | bytes accessed | tf_op | source)
XLA Modules:
  0.0 77.3 jit_solution(13273024600231926477)
XLA Ops:
  0.0 75.4 %shard_map.136 = bf16[128,2048]{1,0:T(8,128)(2,1)} custom-call(bf16[128,2048]{1,0:T(8,128)(2,1)} %tok_hbm.1, f32[1,2048]{1,0:T(1,128)} %bitcast.5, f32[1,128]{1,0:T(1,128)} %bitcast.8, f32[4,128]{1,0:T(4,128)} %bitcast.7, f32[1,64]{1,0:T(1,128)} %bitcast.9, f32[1,2048]{1,0:T(1,128)} %bitcast.6, bf16[64,128]{1,0:T(8,128)(2,1)} %wq.1, bf16[64,128]{1,0:T(8,128)(2,1)} %wk.1, ...), custom_call_target="tpu_custom_call" | custom-call | tf_op jit(solution)/shard_map/pallas_call | solution.py:481
  75.5 1.9 %copy.16 = bf16[128,2048]{1,0:T(8,128)(2,1)} copy(bf16[128,2048]{1,0:T(8,128)(2,1)} %shard_map.136) | data formatting | bytes 1048576

commit v7 on v6

--- a/solution.py
+++ b/solution.py
@@ -146,14 +146,14 @@
     *((f"mix{c}", 0.23, ("attend", 1), (f"d0{c}",)) for c in EACH),
     *((f"pair0{c}", 0.05, (f"d0{c}",), (f"x0{c}",)) for c in EACH),
     *((f"residual{c}", 0.08, (f"x0{c}", *((f"residual{c - 1}",) if c else ())), (f"s0{c}",)) for c in EACH),
-    *((f"relay0{c}", 0.03, (f"s0{c}",), (f"f0{c}",)) for c in EACH),
-    ("gate_up", 1.12, (*(f"f0{c}" for c in EACH), *(f"relay0{c}" for c in EACH), 2), ()),
+    *((f"relay0{c}", 0.03, (f"s0{c}",), ("f00",) if c == CHUNKS - 1 else ()) for c in EACH),
+    ("gate_up", 1.12, ("f00", *(f"relay0{c}" for c in EACH), 2), ()),
     ("hidden", 0.07, ("gate_up",), ()),
     *((f"down{c}", 0.27, ("hidden", *LAST[c]), (f"d1{c}",)) for c in EACH),
     *((f"pair1{c}", 0.05, (f"d1{c}",), (f"x1{c}",)) for c in EACH),
     *((f"layer{c}", 0.05, (f"x1{c}",), (f"s1{c}",)) for c in EACH),
-    *((f"relay1{c}", 0.03, (f"s1{c}",), (f"f1{c}",)) for c in EACH),
-    ("end", 0.1, (*(f"f1{c}" for c in EACH), *(f"relay1{c}" for c in EACH)), ()),
+    *((f"relay1{c}", 0.03, (f"s1{c}",), ("f10",) if c == CHUNKS - 1 else ()) for c in EACH),
+    ("end", 0.1, ("f10", *(f"relay1{c}" for c in EACH)), ()),
 )
 TURN = dict(d=1.3, x=4.9, s=4.4, f=1.3)
 NEAR = 0.3
@@ -377,15 +377,15 @@
         for piece in pieces:
             for k in (1, 2, 3):
                 copy_to(peer(k), 0, piece, piece, trecv.at[0, 2, c])
-            copy_to(partner, 0, piece, piece, trecv.at[0, 3, c])
+            copy_to(partner, 0, piece, piece, trecv.at[0, 3, 0])
 
     def relay_normed(c):
         for k in (1, 2, 3):
             piece = n2.at[around(k), core, :, cols_of(c)]
-            copy_to(partner, 0, piece, piece, trecv.at[0, 3, c])
+            copy_to(partner, 0, piece, piece, trecv.at[0, 3, 0])
             if c == CHUNKS - 1:
                 piece = factors.at[around(k), core]
-                copy_to(partner, 0, piece, piece, trecv.at[0, 3, c])
+                copy_to(partner, 0, piece, piece, trecv.at[0, 3, 0])
 
     def place_of(c):
         return pl.ds(pl.multiple_of(slab_of(c) * (D // NZ), D // NZ), D // NZ)
@@ -396,7 +396,7 @@
 
     def put(i, c):
         piece = fin.at[i, :, cols_of(c)]
-        copy_to(partner, 1, piece, out_at(i, c), trecv.at[1, 3, c])
+        copy_to(partner, 1, piece, out_at(i, c), trecv.at[1, 3, 0])
         pltpu.make_async_copy(piece, out_at(i, c), lsem.at[5]).start()
 
     def layer_out(c):
@@ -416,8 +416,10 @@
     def take_exchange(what):
         n, c = int(what[1]), int(what[2])
         kind = "dxsf".index(what[0])
-        wide = D // CHUNKS + (256 if n == 0 and what[0] in "sf" and c == CHUNKS - 1 else 0)
-        ref = (lands if what[0] in "df" else gots)[n].at[:, :, 0:wide]
+        wide = D // CHUNKS + (256 if n == 0 and what[0] == "s" and c == CHUNKS - 1 else 0)
+        ref = (lands if what[0] == "d" else gots)[n].at[:, :, 0:wide]
+        if what[0] == "f":
+            ref = parts[n].at[:, :, :, 0 : D // 2 + (128 if n == 0 else 0)]
         wait_bytes(ref, trecv.at[n, kind, c])
 
     def gate_up():

time: 77.5 us -> 77.5 us (level)
  no operation moved by 1% of the time
where the time goes in v7:
time: 77.5 us; the launch traced here: 77.3 us
  Pallas kernels  75.4 us (97%)
  local copies, waits for them, and re-layouts  1.88 us (2%)
    pallas_call x1, Pallas kernels, shards(): pl.pallas_call(layer_kernel, out_shape=jax.ShapeDtypeStruct((SEQ, D), BF1...  75.4 us
    unnamed x1, local copies, waits for them, and re-layouts  1.88 us

profile of v7, /device:TPU:1, one launch (start us, length us, event | category | flops | bytes accessed | tf_op | source)
XLA Modules:
  0.0 77.3 jit_solution(6867460432608417800)
XLA Ops:
  0.0 75.4 %shard_map.136 = bf16[128,2048]{1,0:T(8,128)(2,1)} custom-call(bf16[128,2048]{1,0:T(8,128)(2,1)} %tok_hbm.1, f32[1,2048]{1,0:T(1,128)} %bitcast.5, f32[1,128]{1,0:T(1,128)} %bitcast.8, f32[4,128]{1,0:T(4,128)} %bitcast.7, f32[1,64]{1,0:T(1,128)} %bitcast.9, f32[1,2048]{1,0:T(1,128)} %bitcast.6, bf16[64,128]{1,0:T(8,128)(2,1)} %wq.1, bf16[64,128]{1,0:T(8,128)(2,1)} %wk.1, ...), custom_call_target="tpu_custom_call" | custom-call | tf_op jit(solution)/shard_map/pallas_call | solution.py:483
  75.5 1.9 %copy.16 = bf16[128,2048]{1,0:T(8,128)(2,1)} copy(bf16[128,2048]{1,0:T(8,128)(2,1)} %shard_map.136) | data formatting | bytes 1048576
